TPU v7x, 256 devices: a whole 4x4x8 slice. The times are simulated.
256 devices in a mesh: sp: 64 (over z, x, core), tp: 4 (over y).
Axes of the slice: x: 4, y: 4, z: 8, core: 2. Of those that a mesh axis runs over, the one named last changes fastest.
Arguments:
- moe_input: bfloat16 [16384, 2048], P('sp'), may hold values from -6 to 6
- cotangent: bfloat16 [16384, 2048], P('sp'), may hold values from -16 to 16
- expert_ids: int32 [16384, 2], P('sp'), may hold values from 0 to 63, as said below
- route_weights: float32 [16384, 2], P('sp'), may hold values from 0.05 to 1
- gate_weight: bfloat16 [64, 2048, 1024], P('sp', None, 'tp'), may hold values from -0.125 to 0.125
- up_weight: bfloat16 [64, 2048, 1024], P('sp', None, 'tp'), may hold values from -0.125 to 0.125
- down_weight: bfloat16 [64, 1024, 2048], P('sp', 'tp'), may hold values from -0.1875 to 0.1875
- out_weight: bfloat16 [2048, 1024], P(None, 'tp'), may hold values from -0.1875 to 0.1875
- mixer_out: bfloat16 [16384, 1024], P('sp', 'tp'), may hold values from -6 to 6
- query_vectors: bfloat16 [16384, 512], P('sp', 'tp'), may hold values from -0.37109375 to 0.37109375
- key_vectors: bfloat16 [16384, 512], P('sp', 'tp'), may hold values from -0.37109375 to 0.37109375
- value_vectors: bfloat16 [16384, 1024], P('sp', 'tp'), may hold values from -6 to 6
- log_decay: float32 [16384, 512], P('sp', 'tp'), may hold values from -2 to 0
Outputs:
- grad_gate: bfloat16 [64, 2048, 1024], P('sp', None, 'tp')
- grad_up: bfloat16 [64, 2048, 1024], P('sp', None, 'tp')
- grad_down: bfloat16 [64, 1024, 2048], P('sp', 'tp')
- grad_out_weight: float32 [2048, 1024], P('sp', 'tp')
- grad_queries: bfloat16 [16384, 512], P('sp', 'tp')
- grad_keys: bfloat16 [16384, 512], P('sp', 'tp')
- grad_values: bfloat16 [16384, 1024], P('sp', 'tp')
- grad_log_decay: float32 [16384, 512], P('sp', 'tp')
Inputs may be any that keep to these rules, and one draw needn't show every extreme that they name: `expert_ids`: each row names two different experts of one group, expert e lying in group e // 16. Each aligned block of 256 rows names every expert exactly 8 times and has equally many rows in each of the 4 groups.
All inputs are finite; a program needn't handle non-finite values.
Results may differ from a plain program's by a relative error of at most 0.01145.
Values may be sent and summed in bfloat16 or wider, within the bound.
A program may use at most 64 MiB of HBM per device.

v0:
```python
import jax
import jax.numpy as jnp
from jax import lax
from jax.sharding import Mesh
from jax.sharding import PartitionSpec as P

KEY_CHANNELS = 64
VAL_DIM = 128
BLOCK = 64
SP = ("sp_0", "sp_1", "sp_2")


HIGHEST = lax.Precision.HIGHEST


def filled_with(shard, identity):
    return jax.tree.map(
        lambda a, e: jnp.broadcast_to(jnp.asarray(e, a.dtype), a.shape), shard, identity
    )


def gathered_once(shard, axis):
    leaves = jax.tree.leaves(shard)
    turns = sorted(range(len(leaves)), key=lambda k: -leaves[k].size)
    width = (1, *leaves[turns[0]].shape)[-1]
    lines = [
        jnp.pad(leaves[k].reshape(-1), (0, -leaves[k].size % width)).reshape(-1, width)
        for k in turns
    ]
    both, at, found = (lax.all_gather(jnp.concatenate(lines), axis), 0, {})
    for k, line in zip(turns, lines):
        slab = both[:, at : at + len(line)].reshape(len(both), -1)
        found[k] = slab[:, : leaves[k].size].reshape(-1, *leaves[k].shape)
        at += len(line)
    numbers = iter(range(len(leaves)))
    return jax.tree.map(lambda _: found[next(numbers)], shard)


def entering(shard, axes, combine, identity):
    before = start = filled_with(shard, identity)
    total = shard
    for axis in reversed(axes):
        devices, place = (lax.axis_size(axis), lax.axis_index(axis))
        pieces = gathered_once(total, axis)
        inside, total = (start, start)
        for k in range(devices):
            passed = k < place
            total = combine(total, jax.tree.map(lambda part: part[k], pieces))
            inside = jax.tree.map(lambda new, old: jnp.where(passed, new, old), total, inside)
        before = combine(inside, before)
    return before


def entering_2(shard, axes, combine, identity):
    before = start = filled_with(shard, identity)
    total = shard
    for axis in reversed(axes):
        devices, place = (lax.axis_size(axis), lax.axis_index(axis))
        pieces = jax.tree.map(lambda part: lax.all_gather(part, axis), total)
        inside, total = (start, start)
        for k in reversed(range(devices)):
            passed = k > place
            total = combine(total, jax.tree.map(lambda part: part[k], pieces))
            inside = jax.tree.map(lambda new, old: jnp.where(passed, new, old), total, inside)
        before = combine(inside, before)
    return before


def side_by_side(arrays, axis, split_dim, concat_dim, along):
    both = jnp.concatenate(arrays, axis=along)
    whole, at, done = (
        lax.all_to_all(both, axis, split_axis=split_dim, concat_axis=concat_dim, tiled=True),
        0,
        [],
    )
    for a in arrays:
        done.append(lax.slice_in_dim(whole, at, at + a.shape[along], axis=along))
        at += a.shape[along]
    return tuple(done)


def sent_together(arrays, axis, dim, along):
    ends, at = ([], 0)
    for a in arrays[:-1]:
        at += a.shape[along]
        ends.append(at)
    both = jnp.concatenate(arrays, axis=along)
    return tuple(jnp.split(lax.all_gather(both, axis, axis=dim, tiled=True), ends, axis=along))


def in_blocks(shard, dim, devices):
    before, after = (shard.shape[:dim], shard.shape[dim + 1 :])
    return jnp.moveaxis(shard.reshape(*before, devices, -1, *after), dim, 0)


def sent_and_summed(shard, axis, dim):
    devices = lax.axis_size(axis)
    pieces = lax.all_to_all(in_blocks(shard, dim, devices), axis, 0, 0, tiled=True)
    return jnp.sum(pieces.astype(jnp.float32), axis=0)


def sent_to_all(shard, axis):
    devices = lax.axis_size(axis)
    return lax.all_to_all(
        jnp.broadcast_to(shard[None], (devices, *shard.shape)), axis, 0, 0, tiled=True
    )


def joined_along(pieces, dim):
    lengths = list(pieces.shape[1:])
    lengths[dim] *= pieces.shape[0]
    return jnp.moveaxis(pieces, 0, dim).reshape(lengths)


def collect(shard, axis, dim):
    pieces = sent_to_all(shard, axis)
    return joined_along(pieces, dim)


def sum_at_owner(shard, axis, dim):
    pieces = in_blocks(shard, dim, lax.axis_size(axis))
    arrived = lax.all_to_all(pieces, axis, split_axis=0, concat_axis=0, tiled=True)
    return arrived.sum(axis=0)


def block_step(memory, inputs):
    query_block, key_block, value_block, decay_block = inputs
    block_len = query_block.shape[1]
    causal = jnp.tril(jnp.ones((block_len, block_len), dtype=bool))
    cumulative = jnp.cumsum(decay_block, axis=1)
    carried = jnp.einsum(
        "hcd,hdv->hcv", query_block * jnp.exp(cumulative), memory, precision=HIGHEST
    )
    difference = cumulative[:, :, None, :] - cumulative[:, None, :, :]
    decay = jnp.exp(jnp.where(causal[None, :, :, None], difference, -jnp.inf))
    scores = jnp.einsum("htd,hsd,htsd->hts", query_block, key_block, decay, precision=HIGHEST)
    within = jnp.einsum("hts,hsv->htv", scores, value_block, precision=HIGHEST)
    final_row = cumulative[:, -1:, :]
    memory = jnp.exp(final_row[:, 0, :])[:, :, None] * memory + jnp.einsum(
        "hsd,hsv->hdv", key_block * jnp.exp(final_row - cumulative), value_block, precision=HIGHEST
    )
    return (memory, carried + within)


def run_blocks(query_heads, key_heads, value_heads, decay_heads, memory):
    head_count = query_heads.shape[0]
    length = query_heads.shape[1]
    block_count = length // BLOCK

    def to_blocks(matrix):
        return matrix.reshape(head_count, block_count, BLOCK, matrix.shape[-1]).transpose(
            1, 0, 2, 3
        )

    memory, outputs = lax.scan(
        jax.checkpoint(block_step),
        memory,
        (
            to_blocks(query_heads),
            to_blocks(key_heads),
            to_blocks(value_heads),
            to_blocks(decay_heads),
        ),
    )
    return (outputs.transpose(1, 0, 2, 3).reshape(head_count, length, outputs.shape[-1]), memory)


def chain_combine(former, latter):
    return (former[0] * latter[0], latter[1] + latter[0][:, :, None] * former[1])


def expert_pass(routed, routed_cot, gate_local, up_local, down_local):
    pre_gate = jnp.dot(routed, gate_local, preferred_element_type=jnp.float32)
    pre_up = jnp.dot(routed, up_local, preferred_element_type=jnp.float32)
    sigmoid_gate = jax.nn.sigmoid(pre_gate)
    activated = pre_gate * sigmoid_gate
    hidden = (activated * pre_up).astype(jnp.bfloat16)
    delta_hidden = jnp.dot(routed_cot, down_local.T, preferred_element_type=jnp.float32)
    grad_down = jnp.dot(hidden.T, routed_cot, preferred_element_type=jnp.float32).astype(
        jnp.bfloat16
    )
    delta_gate = (
        delta_hidden * pre_up * sigmoid_gate * (1.0 + pre_gate * (1.0 - sigmoid_gate))
    ).astype(jnp.bfloat16)
    delta_up = (delta_hidden * activated).astype(jnp.bfloat16)
    grad_gate = jnp.dot(routed.T, delta_gate, preferred_element_type=jnp.float32).astype(
        jnp.bfloat16
    )
    grad_up = jnp.dot(routed.T, delta_up, preferred_element_type=jnp.float32).astype(jnp.bfloat16)
    partial_value = jnp.dot(delta_gate, gate_local.T, preferred_element_type=jnp.float32)
    partial_value = partial_value + jnp.dot(
        delta_up, up_local.T, preferred_element_type=jnp.float32
    )
    return (grad_gate, grad_up, grad_down, partial_value)


def mixer_backward(query_vectors, key_vectors, value_vectors, log_decay, delta_mixer):
    tok_count = query_vectors.shape[0]

    def heads_first(matrix, channel_size):
        return matrix.astype(jnp.float32).reshape(tok_count, -1, channel_size).transpose(1, 0, 2)

    def tokens_first(matrix):
        return matrix.transpose(1, 0, 2).reshape(tok_count, -1)

    query_heads = heads_first(query_vectors, KEY_CHANNELS)
    key_heads = heads_first(key_vectors, KEY_CHANNELS)
    value_heads = heads_first(value_vectors, VAL_DIM)
    decay_heads = heads_first(log_decay, KEY_CHANNELS)
    cot_heads = heads_first(delta_mixer, VAL_DIM)
    cumulative = jnp.cumsum(decay_heads, axis=1)
    decay_total = cumulative[:, -1, :]
    retention = jnp.exp(decay_total)
    local_state = jnp.einsum(
        "hld,hlv->hdv",
        key_heads * jnp.exp(decay_total[:, None, :] - cumulative),
        value_heads,
        precision=HIGHEST,
    )
    local_pull = jnp.einsum(
        "hld,hlv->hdv",
        query_heads * KEY_CHANNELS ** (-0.5) * jnp.exp(cumulative),
        cot_heads,
        precision=HIGHEST,
    )
    identity = (jnp.ones_like(retention), jnp.zeros_like(local_state))
    start_state = entering((retention, local_state), SP, chain_combine, identity)[1]
    end_pull = entering_2((retention, local_pull), SP, chain_combine, identity)[1]

    def local_forward(query_in, key_in, value_in, decay_in):
        return run_blocks(
            query_in * KEY_CHANNELS ** (-0.5), key_in, value_in, decay_in, start_state
        )

    pullback = jax.vjp(local_forward, query_heads, key_heads, value_heads, decay_heads)[1]
    grads = pullback((cot_heads, end_pull))
    return (
        tokens_first(grads[0]).astype(jnp.bfloat16),
        tokens_first(grads[1]).astype(jnp.bfloat16),
        tokens_first(grads[2]).astype(jnp.bfloat16),
        tokens_first(grads[3]),
    )


def shards(
    moe_input,
    cotangent,
    expert_ids,
    route_weights,
    gate_weight,
    up_weight,
    down_weight,
    out_weight,
    mixer_out,
    query_vectors,
    key_vectors,
    value_vectors,
    log_decay,
):
    tok_count = moe_input.shape[0]
    model_width = moe_input.shape[1]
    slot_total = 2 * tok_count
    flat_ids = expert_ids.reshape(-1)
    sorting = jnp.argsort(flat_ids, stable=True)
    source_rows = sorting // 2
    inverse = jnp.argsort(sorting)
    gate_local = gate_weight[0]
    up_local = up_weight[0]
    down_local = down_weight[0]
    quarter = model_width // lax.axis_size("tp")
    offset = lax.axis_index("tp") * quarter
    own_input = lax.dynamic_slice_in_dim(moe_input, offset, quarter, 1)
    own_cot = lax.dynamic_slice_in_dim(cotangent, offset, quarter, 1)
    own_scaled = (route_weights[:, :, None] * own_cot[:, None, :].astype(jnp.float32)).astype(
        jnp.bfloat16
    )
    own_scaled = own_scaled.reshape(slot_total, quarter)
    arrived = side_by_side((own_input[source_rows], own_scaled[sorting]), SP, 0, 0, 1)
    routed, routed_cot = sent_together((arrived[0], arrived[1]), "tp", 1, 0)
    grad_gate, grad_up, grad_down, partial_value = expert_pass(
        routed, routed_cot, gate_local, up_local, down_local
    )
    summed = sent_and_summed(partial_value.astype(jnp.bfloat16), "tp", 1).astype(jnp.bfloat16)
    returned = lax.all_to_all(summed, SP, split_axis=0, concat_axis=0, tiled=True)
    per_slot = returned[inverse].reshape(tok_count, 2, quarter).astype(jnp.float32)
    own_grad = (own_cot.astype(jnp.float32) + per_slot[:, 0] + per_slot[:, 1]).astype(jnp.bfloat16)
    token_grad = collect(own_grad, "tp", 1)
    delta_mixer = jnp.dot(token_grad, out_weight, preferred_element_type=jnp.float32).astype(
        jnp.bfloat16
    )
    grad_out_weight = sum_at_owner(
        jnp.dot(token_grad.T, mixer_out, preferred_element_type=jnp.float32), SP, 0
    )
    gradients = mixer_backward(query_vectors, key_vectors, value_vectors, log_decay, delta_mixer)
    return (
        grad_gate[None],
        grad_up[None],
        grad_down[None],
        grad_out_weight,
        gradients[0],
        gradients[1],
        gradients[2],
        gradients[3],
    )


def solution(mesh):
    finer = Mesh(mesh.devices.reshape(8, 4, 2, mesh.shape["tp"]), ("sp_0", "sp_1", "sp_2", "tp"))
    in_specs = (
        P(SP, None),
        P(SP, None),
        P(SP, None),
        P(SP, None),
        P(SP, None, "tp"),
        P(SP, None, "tp"),
        P(SP, "tp", None),
        P(None, "tp"),
        P(SP, "tp"),
        P(SP, "tp"),
        P(SP, "tp"),
        P(SP, "tp"),
        P(SP, "tp"),
    )
    out_specs = (
        P(SP, None, "tp"),
        P(SP, None, "tp"),
        P(SP, "tp", None),
        P(SP, "tp"),
        P(SP, "tp"),
        P(SP, "tp"),
        P(SP, "tp"),
        P(SP, "tp"),
    )
    return jax.shard_map(
        shards, mesh=finer, in_specs=in_specs, out_specs=out_specs, check_vma=False
    )
```

profile of v0, /device:TPU:1, one launch (start us, length us, event | category | flops | bytes accessed | tf_op | source)
XLA Modules:
  0.0 359.3 jit_solution(10521336245124860007)
XLA Ops:
  10.1 3.8 %sort.34 = (s32[512]{0:T(512)}, s32[512]{0:T(512)S(1)}) sort(s32[512]{0:T(512)S(1)} %reshape.478, s32[512]{0:T(512)S(1)} %iota.42), dimensions={0}, to_apply=%region_0.0 | sort | flops 4608 | bytes 8192 | tf_op jit(solution)/shard_map/jit(argsort)/sort | solution.py:264
  18.2 41.1 %all_to_all.39 = bf16[64,8,1024]{2,1,0:T(8,128)(2,1)S(1)} all-to-all(bf16[64,8,1024]{2,1,0:T(8,128)(2,1)S(1)} %maximum_bitcast_fusion), channel_id=1, replica_groups=mesh['sp_0'=8,'sp_1'=4,'sp_2'=2,'tp'=4] {'sp_0','sp_1','sp_2'}, dimensions={0} | all-to-all | bytes 2097152 | tf_op jit(solution)/shard_map/all_to_all | solution.py:72
  60.5 3.8 %sort.35 = (s32[512]{0:T(512)}, s32[512]{0:T(512)}) sort(s32[512]{0:T(512)S(1)} %get-tuple-element.288, s32[512]{0:T(512)S(1)} %iota.43), dimensions={0}, to_apply=%region_2.3 | sort | flops 4608 | bytes 8192 | tf_op jit(solution)/shard_map/jit(argsort)/sort | solution.py:266
  67.1 2.7 all-gather.6
  69.9 10.6 %all-gather.7 = f32[4,129,128]{2,1,0:T(8,128)S(1)} all-gather(f32[1,129,128]{2,1,0:T(8,128)S(1)} %maximum_bitcast_fusion.2), channel_id=5, replica_groups=mesh['sp_0'=8,'sp_1'=4,'sp_2'=2,'tp'=4] {'sp_1'}, dimensions={0}, use_global_device_ids=true | all-gather | bytes 330240 | tf_op jit(solution)/shard_map/all_gather | solution.py:30
  80.7 22.1 %all-gather.8 = f32[8,129,128]{2,1,0:T(8,128)S(1)} all-gather(f32[1,129,128]{2,1,0:T(8,128)S(1)} %maximum_bitcast_fusion.3), channel_id=6, replica_groups=mesh['sp_0'=8,'sp_1'=4,'sp_2'=2,'tp'=4] {'sp_0'}, dimensions={0}, use_global_device_ids=true | all-gather | bytes 594432 | tf_op jit(solution)/shard_map/all_gather | solution.py:30
  107.5 7.0 %all-gather.1 = f32[4,1,64]{2,1,0:T(1,128)S(1)} all-gather(f32[2,1,64]{2,1,0:T(1,128)S(1)} %copy.197), channel_id=3, replica_groups=mesh['sp_0'=8,'sp_1'=4,'sp_2'=2,'tp'=4] {'sp_2'}, dimensions={0}, use_global_device_ids=true | all-gather | bytes 1536 | tf_op jit(solution)/shard_map/all_gather | solution.py:59
  114.5 7.4 %all-gather.5 = f32[8,1,64]{2,1,0:T(1,128)S(1)} all-gather(f32[2,1,64]{2,1,0:T(1,128)S(1)} %get-tuple-element.537), channel_id=7, replica_groups=mesh['sp_0'=8,'sp_1'=4,'sp_2'=2,'tp'=4] {'sp_1'}, dimensions={0}, use_global_device_ids=true | all-gather | bytes 2560 | tf_op jit(solution)/shard_map/all_gather | solution.py:59
  130.6 4.7 %all-to-all-start.1 = ((bf16[4,512,512]{2,1,0:T(8,128)(2,1)}), bf16[4,512,512]{2,1,0:T(8,128)(2,1)S(1)}, u32[]{:S(2)}, u32[]{:S(2)}) async-start(bf16[4,512,512]{2,1,0:T(8,128)(2,1)} %bitcast.486), calls=%async_computation.1 | async-start | bytes 4194304 | tf_op jit(solution)/shard_map/all_to_all | solution.py:98
  135.3 15.5 %while.34 = (s32[]{:T(128)}, f32[2,64,128]{2,1,0:T(8,128)S(1)}, f32[4,2,64,128]{3,2,1,0:T(8,128)}, f32[4,2,64,64]{3,2,1,0:T(8,128)}, f32[4,2,64,64]{2,0,3,1:T(4,...) while((s32[]{:T(128)}, f32[2,64,128]{2,1,0:T(8,128)S(1)}, f32[4,2,64,128]{3,2,1,0:T(8,128)}, ...), condition=%wide.region_8.9_spmd, body=%wide.region_6.8_spmd.sunk | while | flops 13148162 | bytes 658545 | solution.py:155
  150.8 8.2 %all-to-all-done.1 = bf16[4,512,512]{2,1,0:T(8,128)(2,1)S(1)} async-done(((bf16[4,512,512]{2,1,0:T(8,128)(2,1)}), bf16[4,512,512]{2,1,0:T(8,128)(2,1)S(1)}, u32[]{:S(2)}, u32[]{:S(2)}) %all-to-all-start.1) | async-done | bytes 2097184 | tf_op jit(solution)/shard_map/all_to_all | solution.py:98
  160.3 7.6 %all-to-all-start.2 = ((bf16[64,8,512]{2,1,0:T(8,128)(2,1)}), bf16[64,8,512]{2,1,0:T(8,128)(2,1)S(1)}, u32[]{:S(2)}, u32[]{:S(2)}) async-start(bf16[64,8,512]{2,1,0:T(8,128)(2,1)} %bitcast.492), calls=%async_computation.2 | async-start | bytes 1048576 | tf_op jit(solution)/shard_map/all_to_all | solution.py:284
  167.9 21.0 %all_gather.54 = f32[8,2,64]{2,1,0:T(2,128)S(1)} all-gather(f32[1,2,64]{2,1,0:T(2,128)S(1)} %bitcast.544), channel_id=1, replica_groups=mesh['sp_0'=8,'sp_1'=4,'sp_2'=2,'tp'=4] {'sp_0'}, dimensions={0}, use_global_device_ids=true | all-gather | bytes 4608 | tf_op jit(solution)/shard_map/all_gather | solution.py:59
  195.5 3.5 all-to-all-start.3
  199.1 3.5 fusion.25
  206.1 4.3 %all-to-all-done.3 = bf16[4,256,512]{1,2,0:T(8,128)(2,1)S(1)} async-done(((bf16[4,256,512]{1,2,0:T(8,128)(2,1)}), bf16[4,256,512]{1,2,0:T(8,128)(2,1)S(1)}, u32[]{:S(2)}, u32[]{:S(2)}) %all-to-all-start.3) | async-done | bytes 1048608 | tf_op jit(solution)/shard_map/all_to_all | solution.py:104
  212.1 13.6 %all-to-all-start.4 = ((f32[64,32,256]{2,1,0:T(8,128)}), f32[64,32,256]{2,1,0:T(8,128)}, u32[]{:S(2)}, u32[]{:S(2)}) async-start(f32[64,32,256]{2,1,0:T(8,128)} %fusion.49), calls=%async_computation.4 | async-start | bytes 4194304 | tf_op jit(solution)/shard_map/all_to_all | solution.py:122
  230.0 11.7 %all_gather.51 = f32[4,2,64,128]{3,2,1,0:T(8,128)S(1)} all-gather(f32[1,2,64,128]{3,2,1,0:T(8,128)S(1)} %fusion.81), channel_id=1, replica_groups=mesh['sp_0'=8,'sp_1'=4,'sp_2'=2,'tp'=4] {'sp_1'}, dimensions={0}, use_global_device_ids=true | all-gather | bytes 327680 | tf_op jit(solution)/shard_map/all_gather | solution.py:59
  241.9 46.6 %all_gather.53 = f32[8,2,64,128]{3,2,1,0:T(8,128)S(1)} all-gather(f32[1,2,64,128]{3,2,1,0:T(8,128)S(1)} %multiply_add_fusion.1), channel_id=1, replica_groups=mesh['sp_0'=8,'sp_1'=4,'sp_2'=2,'tp'=4] {'sp_0'}, dimensions={0}, use_global_device_ids=true | all-gather | bytes 589824 | tf_op jit(solution)/shard_map/all_gather | solution.py:59
  289.0 57.3 %while.35 = (s32[]{:T(128)}, f32[2,64,128]{2,1,0:T(8,128)S(1)}, f32[4,2,64,64]{3,1,2,0:T(2,128)S(1)}, bf16[4,2,64,64]{3,1,2,0:T(2,128)(2,1)S(1)}, bf16[4,2,64,12...) while((s32[]{:T(128)}, f32[2,64,128]{2,1,0:T(8,128)S(1)}, ...), condition=%wide.region_16.17_spmd, body=%wide.region_9.16_spmd.sunk | while | flops 87216128 | bytes 3923653 | solution.py:155
  293.2 4.1 %fusion.155 = (f32[2,64,64]{2,1,0:T(8,128)S(1)}, f32[2,64,64]{2,1,0:T(8,128)S(1)}, f32[2,64,64]{2,1,0:T(8,128)S(1)}) fusion(f32[2,64,64]{1,2,0:T(8,128)S(1)} %copy.341, f32[2,64,64]{1,2,0:T(8,128)S(1)} %copy.342, f32[2,64,64]{2,1,0:T(8,128)S(1)} %reduce_window_sum.64, f32[2,64,64]{2,1,0:T(8,128)S(1)} %fusion.154, ...), kind=kLoop, calls=%fused_computation.26.clone.1 | loop fusion | flops 5218304 | bytes 233472 | tf_op jit(solution)/shard_map/transpose(jvp())/while/body/eval_jaxpr/checkpoint/reduce_sum | solution.py:134
  307.5 4.1 %fusion.155 = (f32[2,64,64]{2,1,0:T(8,128)S(1)}, f32[2,64,64]{2,1,0:T(8,128)S(1)}, f32[2,64,64]{2,1,0:T(8,128)S(1)}) fusion(f32[2,64,64]{1,2,0:T(8,128)S(1)} %copy.341, f32[2,64,64]{1,2,0:T(8,128)S(1)} %copy.342, f32[2,64,64]{2,1,0:T(8,128)S(1)} %reduce_window_sum.64, f32[2,64,64]{2,1,0:T(8,128)S(1)} %fusion.154, ...), kind=kLoop, calls=%fused_computation.26.clone.1 | loop fusion | flops 5218304 | bytes 233472 | tf_op jit(solution)/shard_map/transpose(jvp())/while/body/eval_jaxpr/checkpoint/reduce_sum | solution.py:134
  321.8 4.1 %fusion.155 = (f32[2,64,64]{2,1,0:T(8,128)S(1)}, f32[2,64,64]{2,1,0:T(8,128)S(1)}, f32[2,64,64]{2,1,0:T(8,128)S(1)}) fusion(f32[2,64,64]{1,2,0:T(8,128)S(1)} %copy.341, f32[2,64,64]{1,2,0:T(8,128)S(1)} %copy.342, f32[2,64,64]{2,1,0:T(8,128)S(1)} %reduce_window_sum.64, f32[2,64,64]{2,1,0:T(8,128)S(1)} %fusion.154, ...), kind=kLoop, calls=%fused_computation.26.clone.1 | loop fusion | flops 5218304 | bytes 233472 | tf_op jit(solution)/shard_map/transpose(jvp())/while/body/eval_jaxpr/checkpoint/reduce_sum | solution.py:134
  336.2 4.1 %fusion.155 = (f32[2,64,64]{2,1,0:T(8,128)S(1)}, f32[2,64,64]{2,1,0:T(8,128)S(1)}, f32[2,64,64]{2,1,0:T(8,128)S(1)}) fusion(f32[2,64,64]{1,2,0:T(8,128)S(1)} %copy.341, f32[2,64,64]{1,2,0:T(8,128)S(1)} %copy.342, f32[2,64,64]{2,1,0:T(8,128)S(1)} %reduce_window_sum.64, f32[2,64,64]{2,1,0:T(8,128)S(1)} %fusion.154, ...), kind=kLoop, calls=%fused_computation.26.clone.1 | loop fusion | flops 5218304 | bytes 233472 | tf_op jit(solution)/shard_map/transpose(jvp())/while/body/eval_jaxpr/checkpoint/reduce_sum | solution.py:134
  (309 shorter events, 104.2 us)
Async XLA Ops:
  7.2 115.2 %copy-start = (bf16[1,2048,256]{2,1,0:T(8,128)(2,1)S(1)}, bf16[1,2048,256]{2,1,0:T(8,128)(2,1)}, u32[]{:S(2)}) copy-start(bf16[1,2048,256]{2,1,0:T(8,128)(2,1)} %param.21) | copy-start | bytes 3145732
  7.2 2.3 copy-start.13
  7.2 2.6 copy-start.14
  7.2 115.2 %all-gather.11.cloned.1.call-start = ((), (), s32[]{:S(2)}) async-start(), calls=%async_computation.5 | async-start | bytes 5242880 | tf_op jit(solution)/shard_map/all_gather | solution.py:88
  18.2 46.1 %copy-start.11 = (bf16[256,128]{1,0:T(8,128)(2,1)S(1)}, bf16[256,128]{1,0:T(8,128)(2,1)}, u32[]{:S(2)}) copy-start(bf16[256,128]{1,0:T(8,128)(2,1)} %param.26) | copy-start | bytes 196612
  18.2 46.2 %copy-start.9 = (f32[256,128]{1,0:T(8,128)S(1)}, f32[256,128]{1,0:T(8,128)}, u32[]{:S(2)}) copy-start(f32[256,128]{1,0:T(8,128)} %param.29) | copy-start | bytes 393220
  18.2 48.2 %copy-start.10 = (bf16[256,256]{1,0:T(8,128)(2,1)S(1)}, bf16[256,256]{1,0:T(8,128)(2,1)}, u32[]{:S(2)}) copy-start(bf16[256,256]{1,0:T(8,128)(2,1)} %param.28) | copy-start | bytes 393220
  18.2 48.3 %copy-start.12 = (bf16[256,128]{1,0:T(8,128)(2,1)S(1)}, bf16[256,128]{1,0:T(8,128)(2,1)}, u32[]{:S(2)}) copy-start(bf16[256,128]{1,0:T(8,128)(2,1)} %param.27) | copy-start | bytes 196612
  106.6 18.3 %copy-start.1 = (f32[256,128]{0,1:T(8,128)}, f32[256,128]{0,1:T(8,128)S(1)}, u32[]{:S(2)}) copy-start(f32[256,128]{0,1:T(8,128)S(1)} %convert_multiply_fusion) | copy-start | bytes 393220
  122.0 2.9 copy-start.3
  122.4 2.9 copy-start.15
  125.3 2.3 copy-start.18
  127.6 1.5 copy-start.4
  130.6 28.5 %all-to-all-start.1 = ((bf16[4,512,512]{2,1,0:T(8,128)(2,1)}), bf16[4,512,512]{2,1,0:T(8,128)(2,1)S(1)}, u32[]{:S(2)}, u32[]{:S(2)}) async-start(bf16[4,512,512]{2,1,0:T(8,128)(2,1)} %bitcast.486), calls=%async_computation.1 | async-start | bytes 4194304 | tf_op jit(solution)/shard_map/all_to_all | solution.py:98
  160.3 29.4 %all-to-all-start.2 = ((bf16[64,8,512]{2,1,0:T(8,128)(2,1)}), bf16[64,8,512]{2,1,0:T(8,128)(2,1)S(1)}, u32[]{:S(2)}, u32[]{:S(2)}) async-start(bf16[64,8,512]{2,1,0:T(8,128)(2,1)} %bitcast.492), calls=%async_computation.2 | async-start | bytes 1048576 | tf_op jit(solution)/shard_map/all_to_all | solution.py:284
  192.4 6.6 %copy-start.5 = (bf16[512,256]{1,0:T(8,128)(2,1)S(1)}, bf16[512,256]{1,0:T(8,128)(2,1)}, u32[]{:S(2)}) copy-start(bf16[512,256]{1,0:T(8,128)(2,1)} %copy-done.4) | copy-start | bytes 786436
  195.5 14.9 %all-to-all-start.3 = ((bf16[4,256,512]{1,2,0:T(8,128)(2,1)}), bf16[4,256,512]{1,2,0:T(8,128)(2,1)S(1)}, u32[]{:S(2)}, u32[]{:S(2)}) async-start(bf16[4,256,512]{1,2,0:T(8,128)(2,1)} %broadcast_in_dim.126), calls=%async_computation.3 | async-start | bytes 2097152 | tf_op jit(solution)/shard_map/all_to_all | solution.py:104
  199.0 3.5 copy-start.7
  199.0 3.5 copy-start.16
  202.5 1.8 copy-start.19
  202.5 1.8 copy-start.21
  204.3 6.1 %copy-start.8 = (bf16[256,256]{1,0:T(8,128)(2,1)S(1)}, bf16[256,256]{1,0:T(8,128)(2,1)}, u32[]{:S(2)}) copy-start(bf16[256,256]{1,0:T(8,128)(2,1)} %param.25) | copy-start | bytes 393220
  212.1 15.4 %copy-start.2 = (f32[256,128]{0,1:T(8,128)S(1)}, f32[256,128]{0,1:T(8,128)}, u32[]{:S(2)}) copy-start(f32[256,128]{0,1:T(8,128)} %copy-done.1) | copy-start | bytes 393220
  212.1 138.0 %all-to-all-start.4 = ((f32[64,32,256]{2,1,0:T(8,128)}), f32[64,32,256]{2,1,0:T(8,128)}, u32[]{:S(2)}, u32[]{:S(2)}) async-start(f32[64,32,256]{2,1,0:T(8,128)} %fusion.49), calls=%async_computation.4 | async-start | bytes 4194304 | tf_op jit(solution)/shard_map/all_to_all | solution.py:122
  (3 other events, 3.8 us)
Sparse Core Ops, SparseCore 0:
  60.5 47.7 all-gather.10
where the time goes:
time: 365 us; the launch traced here: 359 us
  blocking collectives  172 us (47%)
  other arithmetic  56.7 us (16%)
  local copies, waits for them, and re-layouts  45.6 us (12%)
  starting transfers between devices  29.4 us (8%)
  matrix products  27 us (7%)
  between operations  14.9 us (4%)
  waiting for transfers between devices  12.6 us (3%)
    all_gather x6, blocking collectives, entering_2(): pieces = jax.tree.map(lambda part: lax.all_gather(part, axis), total)  95.8 us
    all_to_all x1, blocking collectives, side_by_side(): lax.all_to_all(both, axis, split_axis=split_dim, concat_axis=concat_dim,...  41.1 us
    all_gather x3, blocking collectives, gathered_once(): both, at, found = (lax.all_gather(jnp.concatenate(lines), axis), 0, {})  35.4 us
    reduce_sum x4, other arithmetic, block_step(): difference = cumulative[:, :, None, :] - cumulative[:, None, :, :]  16.3 us
    while x8, other arithmetic  16 us
    all_to_all x1, starting transfers between devices, sum_at_owner(): lax.all_to_all(pieces, axis, split_axis=0, concat_axis=0, tiled=True)  13.6 us
    squeeze x16, local copies, waits for them, and re-layouts, run_blocks(): lax.scan(jax.checkpoint(block_step), memory, (to_blocks(query_heads), to_...  10.4 us
    dynamic_slice x20, local copies, waits for them, and re-layouts, run_blocks(): lax.scan(jax.checkpoint(block_step), memory, (to_blocks(query_heads), to_...  9.79 us
  transfers between devices with their start and end apart: 5, of which 2 were waited for; matrix products, arithmetic and copies ran while one was open for 27% of the time, Pallas kernels for 0%

commit v1 on v0

v1 whole, which is shorter than its diff:
```python
import jax
import jax.numpy as jnp
from jax import lax
from jax.experimental import pallas as pl
from jax.experimental.pallas import tpu as pltpu
from jax.sharding import Mesh
from jax.sharding import PartitionSpec as P

MESH = pl.DeviceIdType.MESH
SP = ("sp_0", "sp_1", "sp_2")
BF16 = jnp.bfloat16
F32 = jnp.float32
NY = 4
BLOCK = 64
VMEM = pl.BlockSpec(memory_space=pltpu.VMEM)
ANY = pl.BlockSpec(memory_space=pl.ANY)


def sizes():
    return lax.axis_size("sp_0"), lax.axis_size("sp_1")


def params(collective_id=None):
    if collective_id is None:
        return pltpu.CompilerParams(vmem_limit_bytes=60 * 1024 * 1024)
    return pltpu.CompilerParams(
        collective_id=collective_id, has_side_effects=True, vmem_limit_bytes=60 * 1024 * 1024
    )


def dot(a, b, ca, cb):
    return lax.dot_general(a, b, (((ca,), (cb,)), ((), ())), preferred_element_type=F32)


def place():
    return (
        lax.axis_index("sp_0"),
        lax.axis_index("sp_1"),
        lax.axis_index("sp_2"),
        lax.axis_index("tp"),
    )


def target(nx, zz, row, y):
    return (zz, row // 2, row % 2, y)


def offset(k):
    return jnp.where(k % 2 == 1, (k + 1) // 2, -(k // 2))


def settle(ref, sem):
    pltpu.make_async_copy(ref, ref, sem).wait()


def greet_plane(nz, nx, z, row, y, sides):
    barrier = pltpu.get_barrier_semaphore()
    rows = 2 * nx
    me = z * rows + row

    def hello(i, carry):
        peer = lax.rem(me + i, nz * rows)
        pl.semaphore_signal(
            barrier,
            inc=1,
            device_id=target(nx, peer // rows, lax.rem(peer, rows), y),
            device_id_type=MESH,
        )
        return carry

    lax.fori_loop(1, nz * rows, hello, 0)
    count = nz * rows - 1
    if sides:
        for side in (1, NY - 1):
            pl.semaphore_signal(
                barrier,
                inc=1,
                device_id=target(nx, z, row, lax.rem(y + side, NY)),
                device_id_type=MESH,
            )
        count += 2
    pl.semaphore_wait(barrier, count)


def remote(src, dst, send_sem, recv_sem, device):
    copy = pltpu.make_async_remote_copy(
        src_ref=src,
        dst_ref=dst,
        send_sem=send_sem,
        recv_sem=recv_sem,
        device_id=device,
        device_id_type=MESH,
    )
    copy.start()


def route_kernel(ids_ref, weights_ref, moe_ref, cot_ref, send_ref, pick_ref, own_ref, moe_q, cot_q, sem):
    tok, quarter = moe_q.shape
    slots = 2 * tok
    y = lax.axis_index("tp")
    cols = pl.ds(pl.multiple_of(y * quarter, quarter), quarter)
    first = pltpu.make_async_copy(moe_ref.at[:, cols], moe_q, sem.at[0])
    second = pltpu.make_async_copy(cot_ref.at[:, cols], cot_q, sem.at[1])
    first.start()
    second.start()
    experts = send_ref.shape[0]
    per = slots // experts
    lanes = max(128, experts)
    which = lax.broadcasted_iota(jnp.int32, (tok, lanes), 1)
    hot = [(ids_ref[:, j : j + 1] == which).astype(F32) for j in range(2)]
    lower = (
        lax.broadcasted_iota(jnp.int32, (tok, tok), 1)
        < lax.broadcasted_iota(jnp.int32, (tok, tok), 0)
    ).astype(BF16)
    before = dot(lower, (hot[0] + hot[1]).astype(BF16), 1, 0)
    slot_iota = lax.broadcasted_iota(jnp.int32, (tok, slots), 1)
    picks = []
    for j in range(2):
        rank = jnp.sum(before * hot[j], axis=1, keepdims=True).astype(jnp.int32)
        slot = ids_ref[:, j : j + 1] * per + rank
        picks.append((slot == slot_iota).astype(BF16))
    both = picks[0] + picks[1]
    pick_ref[...] = both
    first.wait()
    rows = dot(both, moe_q[...], 0, 0).astype(BF16)
    send_ref[:, :, 0:quarter] = rows.reshape(experts, per, quarter)
    second.wait()
    cot = cot_q[...]
    own_ref[...] = cot
    cot32 = cot.astype(F32)
    total = jnp.zeros((slots, quarter), F32)
    for j in range(2):
        scaled = (weights_ref[:, j : j + 1] * cot32).astype(BF16)
        total = total + dot(picks[j], scaled, 0, 0)
    send_ref[:, :, quarter:] = total.astype(BF16).reshape(experts, per, quarter)


def route(ids, weights, moe, cot):
    nz, nx = sizes()
    experts = nz * nx * 2
    tok, width = moe.shape
    quarter = width // NY
    per = 2 * tok // experts
    return pl.pallas_call(
        route_kernel,
        name="route",
        out_shape=(
            jax.ShapeDtypeStruct((experts, per, 2 * quarter), BF16),
            jax.ShapeDtypeStruct((tok, 2 * tok), BF16),
            jax.ShapeDtypeStruct((tok, quarter), BF16),
        ),
        in_specs=[VMEM, VMEM, ANY, ANY],
        out_specs=(VMEM, VMEM, VMEM),
        scratch_shapes=[
            pltpu.VMEM((tok, quarter), BF16),
            pltpu.VMEM((tok, quarter), BF16),
            pltpu.SemaphoreType.DMA((2,)),
        ],
        compiler_params=params(),
    )(ids, weights, moe, cot)


def dispatch_kernel(nz, nx, send_ref, out_ref, own_sem, send_sem, ring_sem, come, from_l, from_r, far_l, far_r):
    z, x, c, y = place()
    rows = 2 * nx
    row = x * 2 + c
    me = z * rows + row
    half = rows // 2
    right = target(nx, z, row, lax.rem(y + 1, NY))
    left = target(nx, z, row, lax.rem(y + NY - 1, NY))
    y_left, y_right = lax.rem(y + NY - 1, NY), lax.rem(y + 1, NY)
    greet_plane(nz, nx, z, row, y, True)
    own = pltpu.make_async_copy(send_ref.at[me], out_ref.at[y, me], own_sem)
    own.start()

    def scatter(i, carry):
        k, j = i // rows, lax.rem(i, rows)
        zz = lax.rem(z - offset(k) + nz, nz)
        to = lax.rem(row + j, rows)
        remote(
            send_ref.at[zz * rows + to],
            out_ref.at[y, me],
            send_sem,
            come.at[k],
            target(nx, zz, to, y),
        )
        return carry

    lax.fori_loop(1, nz * rows, scatter, 0)
    own.wait()

    def spread(k):
        part = pl.ds(lax.rem(z + offset(k) + nz, nz) * rows, rows)
        block = out_ref.at[y, part]
        remote(block, block, ring_sem, from_l.at[k], right)
        remote(block, block, ring_sem, from_r.at[k], left)

    def onward(k):
        at = lax.rem(z + offset(k) + nz, nz) * rows
        settle(out_ref.at[y_left, pl.ds(at, rows)], from_l.at[k])
        block = out_ref.at[y_left, pl.ds(at, half)]
        remote(block, block, ring_sem, far_l.at[k], right)
        settle(out_ref.at[y_right, pl.ds(at, rows)], from_r.at[k])
        block = out_ref.at[y_right, pl.ds(at + half, half)]
        remote(block, block, ring_sem, far_r.at[k], left)

    settle(out_ref.at[y, pl.ds(0, rows - 1)], come.at[0])
    spread(0)

    def step(k, carry):
        settle(out_ref.at[y, pl.ds(0, rows)], come.at[k])
        spread(k)
        onward(k - 1)
        return carry

    lax.fori_loop(1, nz, step, 0)
    onward(nz - 1)

    def finish(k, carry):
        settle(out_ref.at[y, pl.ds(0, half)], far_l.at[k])
        settle(out_ref.at[y, pl.ds(0, half)], far_r.at[k])
        return carry

    lax.fori_loop(0, nz, finish, 0)
    settle(send_ref.at[pl.ds(0, nz * rows - 1)], send_sem)
    settle(out_ref.at[pl.ds(0, 3)], ring_sem)


def dispatch(send):
    nz, nx = sizes()
    experts, per, width = send.shape

    def body(*refs):
        dispatch_kernel(nz, nx, *refs)

    return pl.pallas_call(
        body,
        name="dispatch",
        out_shape=jax.ShapeDtypeStruct((NY, experts, per, width), BF16),
        in_specs=[VMEM],
        out_specs=VMEM,
        scratch_shapes=[pltpu.SemaphoreType.DMA] * 3 + [pltpu.SemaphoreType.DMA((nz,))] * 5,
        compiler_params=params(1),
    )(send)


def expert_kernel(rows_ref, gate_ref, up_ref, down_ref, g_gate, g_up, g_down, part_ref):
    quarter = part_ref.shape[2]
    slots, units = rows_ref.shape[1], gate_ref.shape[1]
    pre_gate = jnp.zeros((slots, units), F32)
    pre_up = jnp.zeros((slots, units), F32)
    delta = jnp.zeros((slots, units), F32)
    for q in range(NY):
        cols = slice(q * quarter, (q + 1) * quarter)
        routed = rows_ref[q, :, 0:quarter]
        pre_gate = pre_gate + dot(routed, gate_ref[cols, :], 1, 0)
        pre_up = pre_up + dot(routed, up_ref[cols, :], 1, 0)
        delta = delta + dot(rows_ref[q, :, quarter:], down_ref[:, cols], 1, 1)
    sig = jax.nn.sigmoid(pre_gate)
    act = pre_gate * sig
    hidden = (act * pre_up).astype(BF16)
    d_gate = (delta * pre_up * sig * (1.0 + pre_gate * (1.0 - sig))).astype(BF16)
    d_up = (delta * act).astype(BF16)
    for q in range(NY):
        cols = slice(q * quarter, (q + 1) * quarter)
        part = dot(d_gate, gate_ref[cols, :], 1, 1) + dot(d_up, up_ref[cols, :], 1, 1)
        part_ref[q] = part.astype(BF16)
    for q in range(NY):
        cols = slice(q * quarter, (q + 1) * quarter)
        routed = rows_ref[q, :, 0:quarter]
        g_gate[cols, :] = dot(routed, d_gate, 0, 0).astype(BF16)
        g_up[cols, :] = dot(routed, d_up, 0, 0).astype(BF16)
        g_down[:, cols] = dot(hidden, rows_ref[q, :, quarter:], 0, 0).astype(BF16)


def expert(rows, gate, up, down):
    _, slots, width = rows.shape
    return pl.pallas_call(
        expert_kernel,
        name="expert",
        out_shape=(
            jax.ShapeDtypeStruct(gate.shape, BF16),
            jax.ShapeDtypeStruct(up.shape, BF16),
            jax.ShapeDtypeStruct(down.shape, BF16),
            jax.ShapeDtypeStruct((NY, slots, width // 2), BF16),
        ),
        in_specs=[VMEM] * 4,
        out_specs=(VMEM,) * 4,
        compiler_params=params(),
    )(rows, gate, up, down)


def giveback_kernel(
    nz, nx, part_ref, out_ref, near_l, near_r, sum_l, sum_r, last_l, last_r, done,
    own_sem, home_sem, ring_sem, ret_sem, a_l, a_r, b_l, b_r,
):
    z, x, c, y = place()
    rows = 2 * nx
    row = x * 2 + c
    me = z * rows + row
    half = rows // 2
    y_left, y_right = lax.rem(y + NY - 1, NY), lax.rem(y + 1, NY)
    y_far = lax.rem(y + 2, NY)
    right = target(nx, z, row, y_right)
    left = target(nx, z, row, y_left)
    greet_plane(nz, nx, z, row, y, True)

    def start_of(k):
        return lax.rem(z + offset(nz - 1 - k) + nz, nz) * rows

    def first(k, carry):
        at = start_of(k)
        remote(part_ref.at[y_far, pl.ds(at, half)], near_l.at[k], ring_sem, a_l.at[k], right)
        remote(part_ref.at[y_far, pl.ds(at + half, half)], near_r.at[k], ring_sem, a_r.at[k], left)
        return carry

    lax.fori_loop(0, nz, first, 0)

    def second(k):
        at = start_of(k)
        remote(
            part_ref.at[y_right, pl.ds(at + half, half)],
            last_l.at[k, pl.ds(half, half)], ring_sem, b_l.at[k], right,
        )
        remote(
            part_ref.at[y_left, pl.ds(at, half)],
            last_r.at[k, pl.ds(0, half)], ring_sem, b_r.at[k], left,
        )
        settle(near_l.at[k], a_l.at[k])
        sum_r[k] = (
            part_ref[y_right, pl.ds(at, half)].astype(F32) + near_l[k].astype(F32)
        ).astype(BF16)
        remote(sum_r.at[k], last_l.at[k, pl.ds(0, half)], ring_sem, b_l.at[k], right)
        settle(near_r.at[k], a_r.at[k])
        sum_l[k] = (
            part_ref[y_left, pl.ds(at + half, half)].astype(F32) + near_r[k].astype(F32)
        ).astype(BF16)
        remote(sum_l.at[k], last_r.at[k, pl.ds(half, half)], ring_sem, b_r.at[k], left)

    def third(k):
        at = start_of(k)
        settle(last_l.at[k], b_l.at[k])
        settle(last_r.at[k], b_r.at[k])
        done[k] = (
            part_ref[y, pl.ds(at, rows)].astype(F32)
            + last_l[k].astype(F32)
            + last_r[k].astype(F32)
        ).astype(BF16)

    def home(k, j):
        zz = lax.rem(z + offset(nz - 1 - k) + nz, nz)
        to = lax.rem(row + j, rows)
        remote(done.at[k, to], out_ref.at[me], home_sem, ret_sem, target(nx, zz, to, y))

    second(0)

    def step(k, carry):
        second(k)
        third(k - 1)

        def one(j, inner):
            home(k - 1, j)
            return inner

        lax.fori_loop(0, rows, one, 0)
        return carry

    lax.fori_loop(1, nz, step, 0)
    third(nz - 1)

    def one_last(j, inner):
        home(nz - 1, j)
        return inner

    lax.fori_loop(1, rows, one_last, 0)
    own = pltpu.make_async_copy(done.at[nz - 1, row], out_ref.at[me], own_sem)
    own.start()
    own.wait()
    settle(out_ref.at[pl.ds(0, nz * rows - 1)], ret_sem)
    settle(out_ref.at[pl.ds(0, nz * rows - 1)], home_sem)
    settle(part_ref.at[pl.ds(0, 3)], ring_sem)


def giveback(part):
    nz, nx = sizes()
    _, experts, per, quarter = part.shape
    rows = 2 * nx
    half = rows // 2

    def body(*refs):
        giveback_kernel(nz, nx, *refs)

    return pl.pallas_call(
        body,
        name="giveback",
        out_shape=jax.ShapeDtypeStruct((experts, per, quarter), BF16),
        in_specs=[VMEM],
        out_specs=VMEM,
        scratch_shapes=[pltpu.VMEM((nz, half, per, quarter), BF16)] * 4
        + [pltpu.VMEM((nz, rows, per, quarter), BF16)] * 3
        + [pltpu.SemaphoreType.DMA] * 4
        + [pltpu.SemaphoreType.DMA((nz,))] * 4,
        compiler_params=params(2),
    )(part)


def collect_kernel(nx, pick_ref, ret_ref, own_ref, out_ref, ring_sem, from_l, from_r, far_l, far_r):
    z, x, c, y = place()
    row = x * 2 + c
    pieces, span = out_ref.shape[1], out_ref.shape[2]
    half = span // 2
    y_left, y_right = lax.rem(y + NY - 1, NY), lax.rem(y + 1, NY)
    right = target(nx, z, row, y_right)
    left = target(nx, z, row, y_left)
    barrier = pltpu.get_barrier_semaphore()
    pl.semaphore_signal(barrier, inc=1, device_id=left, device_id_type=MESH)
    pl.semaphore_signal(barrier, inc=1, device_id=right, device_id_type=MESH)
    pl.semaphore_wait(barrier, 2)
    for i in range(pieces):
        lines = slice(i * span, (i + 1) * span)
        both = dot(pick_ref[lines, :], ret_ref[...], 1, 0)
        out_ref[y, i] = (own_ref[lines, :].astype(F32) + both).astype(BF16)
        block = out_ref.at[y, i]
        remote(block, block, ring_sem, from_l.at[i], right)
        remote(block, block, ring_sem, from_r.at[i], left)

    def onward(i, carry):
        settle(out_ref.at[y_left, i], from_l.at[i])
        block = out_ref.at[y_left, i, pl.ds(0, half)]
        remote(block, block, ring_sem, far_l.at[i], right)
        settle(out_ref.at[y_right, i], from_r.at[i])
        block = out_ref.at[y_right, i, pl.ds(half, half)]
        remote(block, block, ring_sem, far_r.at[i], left)
        return carry

    lax.fori_loop(0, pieces, onward, 0)

    def finish(i, carry):
        settle(out_ref.at[y, i, pl.ds(0, half)], far_l.at[i])
        settle(out_ref.at[y, i, pl.ds(0, half)], far_r.at[i])
        return carry

    lax.fori_loop(0, pieces, finish, 0)
    settle(out_ref.at[pl.ds(0, 3)], ring_sem)


def collect(pick, returned, own):
    _, nx = sizes()
    tok, quarter = own.shape
    pieces = 4

    def body(*refs):
        collect_kernel(nx, *refs)

    return pl.pallas_call(
        body,
        name="collect",
        out_shape=jax.ShapeDtypeStruct((NY, pieces, tok // pieces, quarter), BF16),
        in_specs=[VMEM] * 3,
        out_specs=VMEM,
        scratch_shapes=[pltpu.SemaphoreType.DMA] + [pltpu.SemaphoreType.DMA((pieces,))] * 4,
        compiler_params=params(3),
    )(pick, returned, own)


def triangle(kind):
    row = lax.broadcasted_iota(jnp.int32, (BLOCK, BLOCK), 0)
    col = lax.broadcasted_iota(jnp.int32, (BLOCK, BLOCK), 1)
    return {"le": col <= row, "ge": col >= row, "lt": col < row}[kind]


def spread_sum(tri, value):
    high = value.astype(BF16)
    rest = value - high.astype(F32)
    mid = rest.astype(BF16)
    low = (rest - mid.astype(F32)).astype(BF16)
    both = jnp.concatenate([high, mid, low], axis=0)
    return dot(jnp.concatenate([tri, tri, tri], axis=1), both, 1, 0)


def diagonal(shape):
    return (lax.broadcasted_iota(jnp.int32, shape, 0) < shape[0] // 2) == (
        lax.broadcasted_iota(jnp.int32, shape, 1) < shape[1] // 2
    )


def local_kernel(
    tg_ref, ow_ref, mix_ref, q_ref, k_ref, v_ref, ld_ref, cot_ref, gw_ref, pay_ref, cum_ref
):
    tok = q_ref.shape[0]
    quarter = tg_ref.shape[2]
    total = jnp.zeros((tok, ow_ref.shape[1]), F32)
    for q in range(NY):
        total = total + dot(tg_ref[q], ow_ref[q * quarter : (q + 1) * quarter, :], 1, 0)
    cot_ref[...] = total.astype(BF16)
    lines = gw_ref.shape[3]
    nz, nx = gw_ref.shape[2], gw_ref.shape[1]
    mix = mix_ref[...]
    for q in range(NY):
        grad = dot(tg_ref[q], mix, 0, 0).astype(BF16)
        for m in range(quarter // lines):
            sp = q * (quarter // lines) + m
            gw_ref[sp % 2, (sp // 2) % nx, sp // (2 * nx)] = grad[m * lines : (m + 1) * lines, :]
    tri = triangle("le").astype(BF16)
    blocks = tok // BLOCK
    same = diagonal((2 * 128, 128))
    state = jnp.zeros((256, 128), F32)
    ends = []
    for b in range(blocks):
        at = slice(b * BLOCK, (b + 1) * BLOCK)
        cum = spread_sum(tri, ld_ref[at, :])
        cum_ref[at, :] = cum
        end = cum[BLOCK - 1 : BLOCK, :]
        ends.append(end)
        kept = (k_ref[at, :].astype(F32) * jnp.exp(end - cum)).astype(BF16)
        state = state * jnp.exp(end) + dot(v_ref[at, :], kept, 0, 0)
    pull = jnp.zeros((256, 128), F32)
    for b in reversed(range(blocks)):
        at = slice(b * BLOCK, (b + 1) * BLOCK)
        asked = (q_ref[at, :].astype(F32) * 0.125 * jnp.exp(cum_ref[at, :])).astype(BF16)
        pull = pull * jnp.exp(ends[b]) + dot(cot_ref[at, :], asked, 0, 0)
    state = jnp.where(same, state, 0.0)
    pull = jnp.where(same, pull, 0.0)
    state = state[0:128] + state[128:256]
    pull = pull[0:128] + pull[128:256]
    whole = ends[0]
    for b in range(1, blocks):
        whole = whole + ends[b]
    rows = pay_ref.shape[0]
    span = 128 // rows
    for i in range(rows):
        pay_ref[i, 0:span, :] = state[i * span : (i + 1) * span]
        pay_ref[i, span : 2 * span, :] = pull[i * span : (i + 1) * span]
        pay_ref[i, 2 * span :, :] = jnp.broadcast_to(whole, (8, 128))


def local_part(token_grad, out_weight, mixer_out, query, key, value, log_decay):
    nz, nx = sizes()
    rows = 2 * nx
    tok = query.shape[0]
    lines = out_weight.shape[0] // (nz * rows)
    return pl.pallas_call(
        local_kernel,
        name="local",
        out_shape=(
            jax.ShapeDtypeStruct((tok, 256), BF16),
            jax.ShapeDtypeStruct((2, nx, nz, lines, 256), BF16),
            jax.ShapeDtypeStruct((rows, 2 * (128 // rows) + 8, 128), F32),
            jax.ShapeDtypeStruct((tok, 128), F32),
        ),
        in_specs=[VMEM] * 7,
        out_specs=(VMEM,) * 4,
        compiler_params=params(),
    )(token_grad, out_weight, mixer_out, query, key, value, log_decay)


def exchange_kernel(
    nz, nx, pay_ref, gw_ref, ex_ref, gout_ref,
    row_in, z_out, z_in, row_out, core_in, x_out, x_in, last_out, last_in, ends,
    own_sem, sent, p1, p2, p3, g1, g2, g3,
):
    z, x, c, y = place()
    rows = 2 * nx
    row = x * 2 + c
    span = 128 // rows
    barrier = pltpu.get_barrier_semaphore()

    def greet_row(j, carry):
        pl.semaphore_signal(
            barrier, inc=1, device_id=target(nx, z, lax.rem(row + j, rows), y), device_id_type=MESH
        )
        return carry

    def greet_z(j, carry):
        pl.semaphore_signal(
            barrier, inc=1, device_id=target(nx, lax.rem(z + j, nz), row, y), device_id_type=MESH
        )
        return carry

    lax.fori_loop(1, rows, greet_row, 0)
    lax.fori_loop(1, nz, greet_z, 0)
    pl.semaphore_wait(barrier, rows + nz - 2)

    def row_send(j, carry):
        to = lax.rem(row + j, rows)
        remote(pay_ref.at[to], row_in.at[row], sent.at[0], p1, target(nx, z, to, y))
        return carry

    lax.fori_loop(1, rows, row_send, 0)
    remote(gw_ref.at[1 - c], core_in, sent.at[3], g1, (z, x, 1 - c, y))
    own = pltpu.make_async_copy(pay_ref.at[row], row_in.at[row], own_sem)
    own.start()
    own.wait()

    settle(row_in.at[pl.ds(0, rows - 1)], p1)
    state = jnp.zeros((span, 128), F32)
    after = jnp.zeros((1, 128), F32)
    for j in range(rows):
        row_out[j, 0:span, :] = state
        ends[j : j + 1, :] = after
        keep = row_in[j, 2 * span : 2 * span + 1, :]
        state = state * jnp.exp(keep) + row_in[j, 0:span, :]
        after = after + keep
    pull = jnp.zeros((span, 128), F32)
    for j in reversed(range(rows)):
        row_out[j, span : 2 * span, :] = pull
        pull = pull * jnp.exp(row_in[j, 2 * span : 2 * span + 1, :]) + row_in[j, span : 2 * span, :]
    z_out[0:span, :] = state
    z_out[span : 2 * span, :] = pull
    z_out[2 * span :, :] = jnp.broadcast_to(after, (8, 128))
    z_in[z] = z_out[...]

    def z_send(j, carry):
        remote(z_out, z_in.at[z], sent.at[1], p2, target(nx, lax.rem(z + j, nz), row, y))
        return carry

    lax.fori_loop(1, nz, z_send, 0)

    settle(core_in, g1)
    for xx in range(nx):
        x_out[xx] = (gw_ref[c, xx].astype(F32) + core_in[xx].astype(F32)).astype(BF16)

    def x_send(j, carry):
        to = lax.rem(x + j, nx)
        remote(x_out.at[to], x_in.at[x], sent.at[4], g2, (z, to, c, y))
        return carry

    lax.fori_loop(1, nx, x_send, 0)

    settle(z_in.at[pl.ds(0, nz - 1)], p2)
    state = jnp.zeros((span, 128), F32)
    mine = jnp.zeros((span, 128), F32)
    for k in range(nz):
        mine = jnp.where(z == k, state, mine)
        state = state * jnp.exp(z_in[k, 2 * span : 2 * span + 1, :]) + z_in[k, 0:span, :]
    pull = jnp.zeros((span, 128), F32)
    mine_pull = jnp.zeros((span, 128), F32)
    for k in reversed(range(nz)):
        mine_pull = jnp.where(z == k, pull, mine_pull)
        pull = pull * jnp.exp(z_in[k, 2 * span : 2 * span + 1, :]) + z_in[k, span : 2 * span, :]
    behind = jnp.zeros((1, 128), F32)
    for j in reversed(range(rows)):
        row_out[j, 0:span, :] = row_out[j, 0:span, :] + mine * jnp.exp(ends[j : j + 1, :])
        row_out[j, span : 2 * span, :] = row_out[j, span : 2 * span, :] + mine_pull * jnp.exp(behind)
        behind = behind + row_in[j, 2 * span : 2 * span + 1, :]

    def row_back(j, carry):
        to = lax.rem(row + j, rows)
        remote(row_out.at[to], ex_ref.at[row], sent.at[2], p3, target(nx, z, to, y))
        return carry

    lax.fori_loop(1, rows, row_back, 0)
    ex_ref[row] = row_out[row]

    settle(x_in.at[pl.ds(0, nx - 1)], g2)
    total = x_out[x].astype(F32)
    for j in range(1, nx):
        total = total + x_in[lax.rem(x + j, nx)].astype(F32)
    last_out[...] = total.astype(BF16)

    def last_send(j, carry):
        to = lax.rem(z + j, nz)
        remote(last_out.at[to], last_in.at[z], sent.at[5], g3, (to, x, c, y))
        return carry

    lax.fori_loop(1, nz, last_send, 0)
    settle(last_in.at[pl.ds(0, nz - 1)], g3)
    total = last_out[z].astype(F32)
    for j in range(1, nz):
        total = total + last_in[lax.rem(z + j, nz)].astype(F32)
    gout_ref[...] = total

    settle(ex_ref.at[pl.ds(0, rows - 1)], p3)
    settle(pay_ref.at[pl.ds(0, rows - 1)], sent.at[0])
    settle(z_in.at[pl.ds(0, nz - 1)], sent.at[1])
    settle(ex_ref.at[pl.ds(0, rows - 1)], sent.at[2])
    settle(core_in, sent.at[3])
    settle(x_in.at[pl.ds(0, nx - 1)], sent.at[4])
    settle(last_in.at[pl.ds(0, nz - 1)], sent.at[5])


def exchange(pay, gw):
    nz, nx = sizes()
    rows, deep, _ = pay.shape
    lines = gw.shape[3]
    span = 128 // rows

    def body(*refs):
        exchange_kernel(nz, nx, *refs)

    return pl.pallas_call(
        body,
        name="exchange",
        out_shape=(
            jax.ShapeDtypeStruct((rows, 2 * span, 128), F32),
            jax.ShapeDtypeStruct((lines, 256), F32),
        ),
        in_specs=[VMEM, VMEM],
        out_specs=(VMEM, VMEM),
        scratch_shapes=[
            pltpu.VMEM((rows, deep, 128), F32),
            pltpu.VMEM((deep, 128), F32),
            pltpu.VMEM((nz, deep, 128), F32),
            pltpu.VMEM((rows, 2 * span, 128), F32),
            pltpu.VMEM((nx, nz, lines, 256), BF16),
            pltpu.VMEM((nx, nz, lines, 256), BF16),
            pltpu.VMEM((nx, nz, lines, 256), BF16),
            pltpu.VMEM((nz, lines, 256), BF16),
            pltpu.VMEM((nz, lines, 256), BF16),
            pltpu.VMEM((rows, 128), F32),
        ]
        + [pltpu.SemaphoreType.DMA, pltpu.SemaphoreType.DMA((6,))]
        + [pltpu.SemaphoreType.DMA] * 6,
        compiler_params=params(4),
    )(pay, gw)


def attention_kernel(q_ref, k_ref, v_ref, cot_ref, cum_ref, ex_ref, dq_ref, dk_ref, dv_ref, dl_ref, states):
    tok = q_ref.shape[0]
    blocks = tok // BLOCK
    rows = ex_ref.shape[0]
    span = 128 // rows
    same = diagonal((256, 128))
    head0 = lax.broadcasted_iota(jnp.int32, (BLOCK, 128), 1) < 64
    le = triangle("le")
    ge = triangle("ge").astype(BF16)
    lt = triangle("lt").astype(BF16)

    def opened(lower):
        compact = jnp.concatenate([ex_ref[i, lower : lower + span, :] for i in range(rows)], axis=0)
        return jnp.where(same, jnp.concatenate([compact, compact], axis=0), 0.0)

    state = opened(0)
    for b in range(blocks):
        states[b] = state
        if b + 1 < blocks:
            at = slice(b * BLOCK, (b + 1) * BLOCK)
            cum = cum_ref[at, :]
            end = cum[BLOCK - 1 : BLOCK, :]
            kept = (k_ref[at, :].astype(F32) * jnp.exp(end - cum)).astype(BF16)
            state = state * jnp.exp(end) + jnp.where(same, dot(v_ref[at, :], kept, 0, 0), 0.0)
    pull = opened(span)
    for b in reversed(range(blocks)):
        at = slice(b * BLOCK, (b + 1) * BLOCK)
        cum = cum_ref[at, :]
        end = cum[BLOCK - 1 : BLOCK, :]
        middle = cum[BLOCK // 2 - 1 : BLOCK // 2, :]
        query = q_ref[at, :].astype(F32) * 0.125
        key = k_ref[at, :].astype(F32)
        up, down = jnp.exp(cum - middle), jnp.exp(middle - cum)
        q_mid = (query * up).astype(BF16)
        k_mid = (key * down).astype(BF16)
        asked_decay, kept_decay = jnp.exp(cum), jnp.exp(end - cum)
        asked = (query * asked_decay).astype(BF16)
        kept = (key * kept_decay).astype(BF16)
        nothing = jnp.zeros_like(q_mid)
        dq_mid = jnp.zeros((BLOCK, 128), F32)
        dk_mid = jnp.zeros((BLOCK, 128), F32)
        for h in range(2):
            cols = slice(h * 128, (h + 1) * 128)
            mine = head0 if h == 0 else jnp.logical_not(head0)
            q_one = jnp.where(mine, q_mid, nothing)
            k_one = jnp.where(mine, k_mid, nothing)
            cot = cot_ref[at, cols]
            scores = jnp.where(le, dot(q_one, k_one, 1, 1), 0.0).astype(BF16)
            d_scores = jnp.where(le, dot(cot, v_ref[at, cols], 1, 1), 0.0).astype(BF16)
            dq_mid = dq_mid + dot(d_scores, k_one, 1, 0)
            dk_mid = dk_mid + dot(d_scores, q_one, 0, 0)
            dv_ref[at, cols] = (
                dot(scores, cot, 0, 0) + dot(kept, pull[cols, :].astype(BF16), 1, 1)
            ).astype(BF16)
        state = states[b]
        cot = cot_ref[at, :]
        dq_far = dot(cot, state.astype(BF16), 1, 0)
        dk_far = dot(v_ref[at, :], pull.astype(BF16), 1, 0)
        dq_ref[at, :] = ((dq_mid * up + dq_far * asked_decay) * 0.125).astype(BF16)
        dk_ref[at, :] = (dk_mid * down + dk_far * kept_decay).astype(BF16)
        near = q_mid.astype(F32) * dq_mid - k_mid.astype(F32) * dk_mid
        near = near + query * asked_decay * dq_far
        far = key * kept_decay * dk_far
        carried = jnp.sum(state * pull, axis=0, keepdims=True) * jnp.exp(end)
        dl_ref[at, :] = spread_sum(ge, near) + spread_sum(lt, far) + carried
        if b:
            pull = pull * jnp.exp(end) + jnp.where(same, dot(cot, asked, 0, 0), 0.0)


def attention(query, key, value, cot, cum, ex):
    tok = query.shape[0]
    return pl.pallas_call(
        attention_kernel,
        name="attention",
        out_shape=(
            jax.ShapeDtypeStruct((tok, 128), BF16),
            jax.ShapeDtypeStruct((tok, 128), BF16),
            jax.ShapeDtypeStruct((tok, 256), BF16),
            jax.ShapeDtypeStruct((tok, 128), F32),
        ),
        in_specs=[VMEM] * 6,
        out_specs=(VMEM,) * 4,
        scratch_shapes=[pltpu.VMEM((tok // BLOCK, 256, 128), F32)],
        compiler_params=params(),
    )(query, key, value, cot, cum, ex)


def shards(
    moe_input,
    cotangent,
    expert_ids,
    route_weights,
    gate_weight,
    up_weight,
    down_weight,
    out_weight,
    mixer_out,
    query_vectors,
    key_vectors,
    value_vectors,
    log_decay,
):
    tok, width = moe_input.shape
    quarter = width // NY
    send, pick, own_cot = route(expert_ids, route_weights, moe_input, cotangent)
    experts, per, _ = send.shape
    gathered = dispatch(send).reshape(NY, experts * per, 2 * quarter)
    grad_gate, grad_up, grad_down, part = expert(
        gathered, gate_weight[0], up_weight[0], down_weight[0]
    )
    returned = giveback(part.reshape(NY, experts, per, quarter))
    token_grad = collect(pick, returned.reshape(experts * per, quarter), own_cot)
    cot, gw, pay, cum = local_part(
        token_grad.reshape(NY, tok, quarter),
        out_weight,
        mixer_out,
        query_vectors,
        key_vectors,
        value_vectors,
        log_decay,
    )
    ex, grad_out_weight = exchange(pay, gw)
    grads = attention(query_vectors, key_vectors, value_vectors, cot, cum, ex)
    return (
        grad_gate[None],
        grad_up[None],
        grad_down[None],
        grad_out_weight,
        grads[0],
        grads[1],
        grads[2],
        grads[3],
    )


def solution(mesh):
    finer = Mesh(mesh.devices.reshape(8, 4, 2, mesh.shape["tp"]), ("sp_0", "sp_1", "sp_2", "tp"))
    in_specs = (
        P(SP, None),
        P(SP, None),
        P(SP, None),
        P(SP, None),
        P(SP, None, "tp"),
        P(SP, None, "tp"),
        P(SP, "tp", None),
        P(None, "tp"),
        P(SP, "tp"),
        P(SP, "tp"),
        P(SP, "tp"),
        P(SP, "tp"),
        P(SP, "tp"),
    )
    out_specs = (
        P(SP, None, "tp"),
        P(SP, None, "tp"),
        P(SP, "tp", None),
        P(SP, "tp"),
        P(SP, "tp"),
        P(SP, "tp"),
        P(SP, "tp"),
        P(SP, "tp"),
    )
    return jax.shard_map(
        shards, mesh=finer, in_specs=in_specs, out_specs=out_specs, check_vma=False
    )
```

time: 365 us -> 162 us (0.44); the launches traced: 359 us -> 161 us
  blocking collectives: 172 us -> 0 us
  Pallas kernels: 0 us -> 156 us
  other arithmetic: 56.7 us -> 0 us
  local copies, waits for them, and re-layouts: 45.6 us -> 4.32 us
  starting transfers between devices: 29.4 us -> 0 us
  matrix products: 27 us -> 0 us
  between operations: 14.9 us -> 0.67 us
  waiting for transfers between devices: 12.6 us -> 0 us
    pallas_call x0 -> x8, Pallas kernels: none -> 156 us  [the longest x1 60.8 us: dispatch(): pl.pallas_call(body, name='dispatch', out_shape=jax.ShapeDtypeStruct((NY,...]
    all_gather x9 -> x0, blocking collectives: 131 us -> none  [the longest x6 95.8 us: entering_2(): pieces = jax.tree.map(lambda part: lax.all_gather(part, axis), total)]
    all_to_all x1 -> x0, blocking collectives: 41.1 us -> none  [side_by_side(): lax.all_to_all(both, axis, split_axis=split_dim, concat_axis=concat_dim,...]
    all_to_all x4 -> x0, starting transfers between devices: 29.3 us -> none  [the longest x1 13.6 us: sum_at_owner(): lax.all_to_all(pieces, axis, split_axis=0, concat_axis=0, tiled=True)]
    dot_general x40 -> x0, matrix products: 27 us -> none  [the longest x12 6.27 us: block_step(): jnp.einsum('hsd,hsv->hdv', key_block * jnp.exp(final_row - cumulative), v...]
    reduce_sum x14 -> x0, other arithmetic: 20.8 us -> none  [the longest x4 16.3 us: block_step(): difference = cumulative[:, :, None, :] - cumulative[:, None, :, :]]
    while x8 -> x0, other arithmetic: 16 us -> none
    all_to_all x4 -> x0, waiting for transfers between devices: 12.6 us -> none  [the longest x1 8.25 us: sent_and_summed(): lax.all_to_all(in_blocks(shard, dim, devices), axis, 0, 0, tiled=True)]
  transfers between devices with their start and end apart: 5 -> 0, of which waited for: 2 -> 0; matrix products, arithmetic and copies ran while one was open for 27% -> 0% of each run, Pallas kernels for 0% -> 0%
where the time goes in v1:
time: 162 us; the launch traced here: 161 us
  Pallas kernels  156 us (96%)
  local copies, waits for them, and re-layouts  4.32 us (3%)
    pallas_call x1, Pallas kernels, dispatch(): pl.pallas_call(body, name='dispatch', out_shape=jax.ShapeDtypeStruct((NY,...  60.8 us
    pallas_call x1, Pallas kernels, giveback(): pl.pallas_call(body, name='giveback', out_shape=jax.ShapeDtypeStruct((exp...  35.7 us
    pallas_call x1, Pallas kernels, exchange(): pl.pallas_call(body, name='exchange', out_shape=(jax.ShapeDtypeStruct((ro...  24.1 us
    pallas_call x1, Pallas kernels, collect(): pl.pallas_call(body, name='collect', out_shape=jax.ShapeDtypeStruct((NY,...  14 us
    pallas_call x1, Pallas kernels, expert(): pl.pallas_call(expert_kernel, name='expert', out_shape=(jax.ShapeDtypeStr...  9.88 us
    unnamed x3, local copies, waits for them, and re-layouts  4.32 us
    pallas_call x1, Pallas kernels, attention(): pl.pallas_call(attention_kernel, name='attention', out_shape=(jax.ShapeDt...  3.82 us
    pallas_call x1, Pallas kernels, route(): pl.pallas_call(route_kernel, name='route', out_shape=(jax.ShapeDtypeStruc...  3.75 us

profile of v1, /device:TPU:1, one launch (start us, length us, event | category | flops | bytes accessed | tf_op | source)
XLA Modules:
  0.0 160.6 jit_solution(3811874588175886517)
XLA Ops:
  0.6 1.5 copy.21.ids_ref
  2.1 1.5 copy.22.weights_ref
  3.6 3.8 %route.1 = (bf16[64,8,1024]{2,1,0:T(8,128)(2,1)}, bf16[256,512]{1,0:T(8,128)(2,1)}, bf16[256,512]{1,0:T(8,128)(2,1)}) custom-call(s32[256,2]{1,0:T(8,128)} %copy.21.ids_ref, f32[256,2]{1,0:T(8,128)} %copy.22.weights_ref, bf16[256,2048]{1,0:T(8,128)(2,1)} %moe_ref.1, bf16[256,2048]{1,0:T(8,128)(2,1)} %cot_ref.1), custom_call_target="tpu_custom_call" | custom-call | tf_op jit(solution)/shard_map/route/pallas_call | solution.py:144
  7.3 60.8 %dispatch.1 = bf16[4,64,8,1024]{3,2,1,0:T(8,128)(2,1)} custom-call(bf16[64,8,1024]{2,1,0:T(8,128)(2,1)} %get-tuple-element.25.refs_0_), custom_call_target="tpu_custom_call" | custom-call | tf_op jit(solution)/shard_map/dispatch/pallas_call | solution.py:236
  68.1 9.9 %expert.1 = (bf16[2048,256]{1,0:T(8,128)(2,1)}, bf16[2048,256]{1,0:T(8,128)(2,1)}, bf16[256,2048]{1,0:T(8,128)(2,1)}, bf16[4,512,512]{2,1,0:T(8,128)(2,1)}) custom-call(bf16[4,512,1024]{2,1,0:T(8,128)(2,1)} %bitcast.10, bf16[2048,256]{1,0:T(8,128)(2,1)} %bitcast.14, bf16[2048,256]{1,0:T(8,128)(2,1)} %bitcast.15, bf16[256,2048]{1,0:T(8,128)(2,1)} %bitcast.16), custom_call_target="tpu_custom_call" | custom-call | tf_op jit(solution)/shard_map/expert/pallas_call | solution.py:278
  78.0 35.7 %giveback.1 = bf16[64,8,512]{2,1,0:T(8,128)(2,1)} custom-call(bf16[4,64,8,512]{3,2,1,0:T(8,128)(2,1)} %bitcast.12), custom_call_target="tpu_custom_call" | custom-call | tf_op jit(solution)/shard_map/giveback/pallas_call | solution.py:393
  113.7 14.0 %collect.1 = bf16[4,4,64,512]{3,2,1,0:T(8,128)(2,1)} custom-call(bf16[256,512]{1,0:T(8,128)(2,1)} %get-tuple-element.29.refs_0_, bf16[512,512]{1,0:T(8,128)(2,1)} %bitcast.13, bf16[256,512]{1,0:T(8,128)(2,1)} %get-tuple-element.31.refs_2_), custom_call_target="tpu_custom_call" | custom-call | tf_op jit(solution)/shard_map/collect/pallas_call | solution.py:455
  127.8 3.6 %local.1 = (bf16[256,256]{1,0:T(8,128)(2,1)}, bf16[2,4,8,32,256]{4,3,2,1,0:T(8,128)(2,1)}, f32[8,40,128]{2,1,0:T(8,128)}, f32[256,128]{1,0:T(8,128)}) custom-call(bf16[4,256,512]{2,1,0:T(8,128)(2,1)} %bitcast.11, bf16[2048,256]{1,0:T(8,128)(2,1)} %ow_ref.1, bf16[256,256]{1,0:T(8,128)(2,1)} %mix_ref.1, bf16[256,128]{1,0:T(8,128)(2,1)} %q_ref.3, ...), custom_call_target="tpu_custom_call" | custom-call | tf_op jit(solution)/shard_map/local/pallas_call | solution.py:542
  131.4 24.1 %exchange.1 = (f32[8,32,128]{2,1,0:T(8,128)}, f32[32,256]{1,0:T(8,128)}) custom-call(f32[8,40,128]{2,1,0:T(8,128)} %get-tuple-element.32.refs_0_, bf16[2,4,8,32,256]{4,3,2,1,0:T(8,128)(2,1)} %get-tuple-element.33.refs_1_), custom_call_target="tpu_custom_call" | custom-call | tf_op jit(solution)/shard_map/exchange/pallas_call | solution.py:691
  155.5 3.8 %attention.1 = (bf16[256,128]{1,0:T(8,128)(2,1)}, bf16[256,128]{1,0:T(8,128)(2,1)}, bf16[256,256]{1,0:T(8,128)(2,1)}, f32[256,128]{1,0:T(8,128)}) custom-call(bf16[256,128]{1,0:T(8,128)(2,1)} %q_ref.3, bf16[256,128]{1,0:T(8,128)(2,1)} %k_ref.3, bf16[256,256]{1,0:T(8,128)(2,1)} %v_ref.3, bf16[256,256]{1,0:T(8,128)(2,1)} %get-tuple-element.35.cot_ref, ...), custom_call_target="tpu_custom_call" | custom-call | tf_op jit(solution)/shard_map/attention/pallas_call | solution.py:789
  159.3 1.4 copy.24

commit v2 on v0

v2 whole, which is shorter than its diff:
```python
import jax
import jax.numpy as jnp
from jax import lax
from jax.experimental import pallas as pl
from jax.experimental.pallas import tpu as pltpu
from jax.sharding import Mesh
from jax.sharding import PartitionSpec as P

MESH = pl.DeviceIdType.MESH
SP = ("sp_0", "sp_1", "sp_2")
BF16 = jnp.bfloat16
F32 = jnp.float32
NY = 4
TRAIL = 2
ORDER = {8: (0, 2, 6, 3, 5, 4, 1, 7)}
BLOCK = 64
VMEM = pl.BlockSpec(memory_space=pltpu.VMEM)
ANY = pl.BlockSpec(memory_space=pl.ANY)


def sizes():
    return lax.axis_size("sp_0"), lax.axis_size("sp_1")


def params(collective_id=None):
    if collective_id is None:
        return pltpu.CompilerParams(vmem_limit_bytes=60 * 1024 * 1024)
    return pltpu.CompilerParams(
        collective_id=collective_id, has_side_effects=True, vmem_limit_bytes=60 * 1024 * 1024
    )


def dot(a, b, ca, cb):
    return lax.dot_general(a, b, (((ca,), (cb,)), ((), ())), preferred_element_type=F32)


def place():
    return (
        lax.axis_index("sp_0"),
        lax.axis_index("sp_1"),
        lax.axis_index("sp_2"),
        lax.axis_index("tp"),
    )


def target(nx, zz, row, y):
    return (zz, row // 2, row % 2, y)


def offset(k, nz):
    order = ORDER.get(nz, tuple(range(nz)))
    out = 0
    for i, ahead in enumerate(order):
        out = out + jnp.where(k == i, ahead, 0)
    return out


def settle(ref, sem):
    pltpu.make_async_copy(ref, ref, sem).wait()


def greet_plane(barrier, nz, nx, z, row, y):
    rows = 2 * nx
    me = z * rows + row

    def hello(i, carry):
        far = jnp.where(i % 2 == 0, nz * rows // 2 - i // 2, nz * rows // 2 + 1 + i // 2)
        peer = lax.rem(me + far, nz * rows)
        pl.semaphore_signal(
            barrier,
            inc=1,
            device_id=target(nx, peer // rows, lax.rem(peer, rows), y),
            device_id_type=MESH,
        )
        return carry

    lax.fori_loop(0, nz * rows - 1, hello, 0)
    for side in (1, NY - 1):
        pl.semaphore_signal(
            barrier,
            inc=1,
            device_id=target(nx, z, row, lax.rem(y + side, NY)),
            device_id_type=MESH,
        )


def remote(src, dst, send_sem, recv_sem, device):
    copy = pltpu.make_async_remote_copy(
        src_ref=src,
        dst_ref=dst,
        send_sem=send_sem,
        recv_sem=recv_sem,
        device_id=device,
        device_id_type=MESH,
    )
    copy.start()


def triangle(kind):
    row = lax.broadcasted_iota(jnp.int32, (BLOCK, BLOCK), 0)
    col = lax.broadcasted_iota(jnp.int32, (BLOCK, BLOCK), 1)
    return {"le": col <= row, "ge": col >= row, "lt": col < row}[kind]


def spread_sum(tri, value):
    high = value.astype(BF16)
    rest = value - high.astype(F32)
    mid = rest.astype(BF16)
    low = (rest - mid.astype(F32)).astype(BF16)
    both = jnp.concatenate([high, mid, low], axis=0)
    return dot(jnp.concatenate([tri, tri, tri], axis=1), both, 1, 0)


def diagonal(shape):
    return (lax.broadcasted_iota(jnp.int32, shape, 0) < shape[0] // 2) == (
        lax.broadcasted_iota(jnp.int32, shape, 1) < shape[1] // 2
    )


def mega_kernel(r, nz, nx):
    z, x, c, y = place()
    rows = 2 * nx
    row = x * 2 + c
    me = z * rows + row
    half = rows // 2
    tok, quarter = r.moe_q.shape
    experts, per = nz * rows, 2 * tok // (nz * rows)
    slots = 2 * tok
    units = r.gate.shape[1]
    y_left, y_right = lax.rem(y + NY - 1, NY), lax.rem(y + 1, NY)
    y_far = lax.rem(y + 2, NY)
    right = target(nx, z, row, y_right)
    left = target(nx, z, row, y_left)
    cols = pl.ds(pl.multiple_of(y * quarter, quarter), quarter)
    loads = [
        pltpu.make_async_copy(src, dst, r.load_sem.at[i])
        for i, (src, dst) in enumerate(
            (
                (r.moe_hbm.at[:, cols], r.moe_q),
                (r.cot_hbm.at[:, cols], r.cot_q),
                (r.ld_hbm, r.ld),
                (r.k_hbm, r.k),
                (r.v_hbm, r.v),
                (r.gate_hbm, r.gate),
                (r.up_hbm, r.up),
                (r.down_hbm, r.down),
                (r.q_hbm, r.q),
                (r.ow_hbm, r.ow),
                (r.mix_hbm, r.mix),
                (r.moe_hbm, r.moe),
                (r.cot_hbm, r.cot),
            )
        )
    ]
    for load in loads:
        load.start()
    barrier = pltpu.get_barrier_semaphore()
    greet_plane(barrier, nz, nx, z, row, y)

    lanes = max(128, experts)
    which = lax.broadcasted_iota(jnp.int32, (lanes, tok), 0)
    hot = [(r.ids[j : j + 1, :] == which).astype(F32) for j in range(2)]
    earlier = (
        lax.broadcasted_iota(jnp.int32, (tok, tok), 0)
        < lax.broadcasted_iota(jnp.int32, (tok, tok), 1)
    ).astype(BF16)
    before = dot((hot[0] + hot[1]).astype(BF16), earlier, 1, 0)
    slot_iota = lax.broadcasted_iota(jnp.int32, (slots, tok), 0)
    picks = []
    for j in range(2):
        rank = jnp.sum(before * hot[j], axis=0, keepdims=True).astype(jnp.int32)
        slot = r.ids[j : j + 1, :] * per + rank
        picks.append((slot == slot_iota).astype(BF16))
    both = picks[0] + picks[1]
    r.pick[...] = both
    slot_weight = jnp.zeros((slots, 1), F32)
    for j in range(2):
        chosen = picks[j].astype(F32) * r.weights[j : j + 1, :]
        slot_weight = slot_weight + jnp.sum(chosen, axis=1, keepdims=True)
    r.slot_weight[...] = jnp.broadcast_to(slot_weight, (slots, 128))
    loads[0].wait()
    sorted_rows = dot(both, r.moe_q[...], 1, 0).astype(BF16)
    r.send[:, :, 0:quarter] = sorted_rows.reshape(experts, per, quarter)
    loads[1].wait()
    sorted_cot = (dot(both, r.cot_q[...], 1, 0) * slot_weight).astype(BF16)
    r.send[:, :, quarter:] = sorted_cot.reshape(experts, per, quarter)
    pl.semaphore_wait(barrier, nz * rows + 1)

    def scatter(i, carry):
        k, j = i // rows, lax.rem(i, rows)
        zz = lax.rem(z - offset(k, nz) + nz, nz)
        to = lax.rem(row + j, rows)
        remote(
            r.send.at[zz * rows + to],
            r.rows.at[y, k * rows + row],
            r.send_sem,
            r.come.at[k],
            target(nx, zz, to, y),
        )
        return carry

    ring = nz - 1 - TRAIL
    lax.fori_loop(rows, (ring + 1) * rows, scatter, 0)
    lines = rows * per
    loads[11].wait()
    loads[12].wait()
    for i, k in enumerate([0, *range(ring + 1, nz)]):
        zz = lax.rem(z - offset(k, nz) + nz, nz)
        there = pl.ds(pl.multiple_of(zz * lines, lines), lines)
        pick_there = r.pick[there, :]
        weight_there = r.slot_weight[there, 0:1]
        block = slice(i * rows, (i + 1) * rows)
        for q in range(NY):
            part = slice(q * quarter, (q + 1) * quarter)
            value = dot(pick_there, r.moe[:, part], 1, 0).astype(BF16)
            r.full[block, q, :, 0:quarter] = value.reshape(rows, per, quarter)
            value = (dot(pick_there, r.cot[:, part], 1, 0) * weight_there).astype(BF16)
            r.full[block, q, :, quarter:] = value.reshape(rows, per, quarter)

        def scatter_full(j, carry, i=i, k=k, zz=zz):
            to = lax.rem(row + j, rows)
            remote(
                r.full.at[i * rows + to],
                r.rows.at[:, k * rows + row],
                r.full_sem,
                r.come.at[k],
                target(nx, zz, to, y),
            )
            return carry

        lax.fori_loop(0 if i else 1, rows, scatter_full, 0)
    own = pltpu.make_async_copy(r.full.at[row], r.rows.at[:, row], r.own_sem.at[0])
    own.start()
    own.wait()

    blocks = tok // BLOCK
    same = diagonal((256, 128))
    tri = triangle("le").astype(BF16)
    for load in loads[2:5]:
        load.wait()
    state = jnp.zeros((256, 128), F32)
    for b in range(blocks):
        at = slice(b * BLOCK, (b + 1) * BLOCK)
        cum = spread_sum(tri, r.ld[at, :])
        r.cum[at, :] = cum
        end = cum[BLOCK - 1 : BLOCK, :]
        kept = (r.k[at, :].astype(F32) * jnp.exp(end - cum)).astype(BF16)
        added = jnp.where(same, dot(r.v[at, :], kept, 0, 0), 0.0)
        r.added[b] = added
        state = state * jnp.exp(end) + added
        whole = end if b == 0 else whole + end
    state = state[0:128] + state[128:256]
    span = 128 // rows
    for i in range(rows):
        r.f_pay[i, 0:span, :] = state[i * span : (i + 1) * span]
        r.f_pay[i, span:, :] = jnp.broadcast_to(whole, (8, 128))

    def f_send(j, carry):
        to = lax.rem(row + j, rows)
        remote(r.f_pay.at[to], r.f_row_in.at[row], r.f_sent.at[0], r.f1, target(nx, z, to, y))
        return carry

    lax.fori_loop(1, rows, f_send, 0)
    r.f_row_in[row] = r.f_pay[row]

    def kept_row(j):
        return r.f_row_in[j, span : span + 1, :]

    def kept_z(k):
        return r.f_z_in[k, span : span + 1, :]

    def forward_row():
        settle(r.f_row_in.at[pl.ds(0, rows - 1)], r.f1)
        state = jnp.zeros((span, 128), F32)
        after = jnp.zeros((1, 128), F32)
        for j in range(rows):
            r.f_row_out[j] = state
            r.ends[j : j + 1, :] = after
            state = state * jnp.exp(kept_row(j)) + r.f_row_in[j, 0:span, :]
            after = after + kept_row(j)
        r.f_z_out[0:span, :] = state
        r.f_z_out[span:, :] = jnp.broadcast_to(after, (8, 128))
        r.f_z_in[z] = r.f_z_out[...]

        def send(j, carry):
            to = lax.rem(z + j, nz)
            remote(r.f_z_out, r.f_z_in.at[z], r.f_sent.at[1], r.f2, target(nx, to, row, y))
            return carry

        lax.fori_loop(1, nz, send, 0)

    def forward_z():
        settle(r.f_z_in.at[pl.ds(0, nz - 1)], r.f2)
        state = jnp.zeros((span, 128), F32)
        mine = jnp.zeros((span, 128), F32)
        for k in range(nz):
            mine = jnp.where(z == k, state, mine)
            state = state * jnp.exp(kept_z(k)) + r.f_z_in[k, 0:span, :]
        for j in range(rows):
            r.f_row_out[j] = r.f_row_out[j] + mine * jnp.exp(r.ends[j : j + 1, :])

        def send(j, carry):
            to = lax.rem(row + j, rows)
            remote(r.f_row_out.at[to], r.f_ex.at[row], r.f_sent.at[2], r.f3, target(nx, z, to, y))
            return carry

        lax.fori_loop(1, rows, send, 0)
        r.f_ex[row] = r.f_row_out[row]

    for load in loads[5:11]:
        load.wait()

    def chunk(k):
        return pl.ds(k * rows, rows)

    def spread(k):
        block = r.rows.at[y, chunk(k)]
        remote(block, block, r.ring_sem, r.from_l.at[k], right)
        remote(block, block, r.ring_sem, r.from_r.at[k], left)

    def onward(k):
        settle(r.rows.at[y_left, chunk(k)], r.from_l.at[k])
        block = r.rows.at[y_left, pl.ds(k * rows, half)]
        remote(block, block, r.ring_sem, r.far_l.at[k], right)
        settle(r.rows.at[y_right, chunk(k)], r.from_r.at[k])
        block = r.rows.at[y_right, pl.ds(k * rows + half, half)]
        remote(block, block, r.ring_sem, r.far_r.at[k], left)

    def gathered(k):
        settle(r.rows.at[y, pl.ds(0, half)], r.far_l.at[k])
        settle(r.rows.at[y, pl.ds(0, half)], r.far_r.at[k])

    def expert(k):
        pre_gate = jnp.zeros((lines, units), F32)
        pre_up = jnp.zeros((lines, units), F32)
        delta = jnp.zeros((lines, units), F32)
        for q in range(NY):
            part = slice(q * quarter, (q + 1) * quarter)
            routed = r.rows[q, chunk(k), :, 0:quarter].reshape(lines, quarter)
            routed_cot = r.rows[q, chunk(k), :, quarter:].reshape(lines, quarter)
            pre_gate = pre_gate + dot(routed, r.gate[part, :], 1, 0)
            pre_up = pre_up + dot(routed, r.up[part, :], 1, 0)
            delta = delta + dot(routed_cot, r.down[:, part], 1, 1)
        sig = jax.nn.sigmoid(pre_gate)
        act = pre_gate * sig
        d_gate = (delta * pre_up * sig * (1.0 + pre_gate * (1.0 - sig))).astype(BF16)
        d_up = (delta * act).astype(BF16)
        at = pl.ds(pl.multiple_of(k * lines, lines), lines)
        r.hidden[at, :] = (act * pre_up).astype(BF16)
        r.d_gate[at, :] = d_gate
        r.d_up[at, :] = d_up

        def give(i, carry):
            q = lax.rem(y + 2 + i, NY)
            part = pl.ds(pl.multiple_of(q * quarter, quarter), quarter)
            value = dot(d_gate, r.gate[part, :], 1, 1) + dot(d_up, r.up[part, :], 1, 1)
            r.part[q, chunk(k)] = value.astype(BF16).reshape(rows, per, quarter)
            return carry

        give(0, 0)
        remote(
            r.part.at[y_far, pl.ds(k * rows, half)],
            r.near_l.at[k], r.back_sem, r.a_l.at[k], right,
        )
        remote(
            r.part.at[y_far, pl.ds(k * rows + half, half)],
            r.near_r.at[k], r.back_sem, r.a_r.at[k], left,
        )
        lax.fori_loop(1, NY, give, 0)
        remote(
            r.part.at[y_right, pl.ds(k * rows + half, half)],
            r.last_l.at[k, pl.ds(half, half)], r.back_sem, r.b_l.at[k], right,
        )
        remote(
            r.part.at[y_left, pl.ds(k * rows, half)],
            r.last_r.at[k, pl.ds(0, half)], r.back_sem, r.b_r.at[k], left,
        )

    def second(k):
        settle(r.near_l.at[k], r.a_l.at[k])
        r.sum_r[k] = (
            r.part[y_right, pl.ds(k * rows, half)].astype(F32) + r.near_l[k].astype(F32)
        ).astype(BF16)
        remote(r.sum_r.at[k], r.last_l.at[k, pl.ds(0, half)], r.back_sem, r.b_l.at[k], right)
        settle(r.near_r.at[k], r.a_r.at[k])
        r.sum_l[k] = (
            r.part[y_left, pl.ds(k * rows + half, half)].astype(F32) + r.near_r[k].astype(F32)
        ).astype(BF16)
        remote(r.sum_l.at[k], r.last_r.at[k, pl.ds(half, half)], r.back_sem, r.b_r.at[k], left)

    def third(k, begin):
        settle(r.last_l.at[k], r.b_l.at[k])
        settle(r.last_r.at[k], r.b_r.at[k])
        r.done[k] = (
            r.part[y, chunk(k)].astype(F32)
            + r.last_l[k].astype(F32)
            + r.last_r[k].astype(F32)
        ).astype(BF16)
        zz = lax.rem(z + offset(k, nz) + nz, nz)

        def home(j, carry):
            to = lax.rem(row + j, rows)
            remote(r.done.at[k, to], r.ret.at[me], r.home_sem, r.ret_sem, target(nx, zz, to, y))
            return carry

        lax.fori_loop(begin, rows, home, 0)

    def arrive(k):
        settle(r.rows.at[y, pl.ds(0, rows)], r.come.at[k])
        spread(k)

    arrive(1)

    def step(t, carry):
        @pl.when(t + 1 <= ring)
        def _():
            arrive(t + 1)

        @pl.when(t <= ring)
        def _():
            onward(t)

        @pl.when(t == 1)
        def _():
            settle(r.rows.at[0, pl.ds(0, NY * (rows - 1))], r.come.at[0])

        @pl.when((t > 1) & (t <= ring + 1))
        def _():
            gathered(t - 1)

        @pl.when(t > ring + 1)
        def _():
            settle(r.rows.at[0, pl.ds(0, NY * rows)], r.come.at[t - 1])

        expert(t - 1)

        @pl.when(t >= 2)
        def _():
            second(t - 2)

        @pl.when(t == 2)
        def _():
            forward_row()

        @pl.when(t == nz // 2 + 1)
        def _():
            forward_z()

        @pl.when(t == 3)
        def _():
            third(0, 1)
            home = pltpu.make_async_copy(r.done.at[0, row], r.ret.at[me], r.own_sem.at[1])
            home.start()
            home.wait()

        @pl.when(t >= 4)
        def _():
            third(t - 3, 0)

        return carry

    lax.fori_loop(1, nz + 1, step, 0)

    def routed_of(q, lower):
        return r.rows[q, :, :, lower : lower + quarter].reshape(slots, quarter)

    def grads(kind, q):
        part = slice(q * quarter, (q + 1) * quarter)
        if kind == "down":
            r.g_down[:, part] = dot(r.hidden[...], routed_of(q, quarter), 0, 0).astype(BF16)
        else:
            routed = routed_of(q, 0)
            r.g_gate[part, :] = dot(routed, r.d_gate[...], 0, 0).astype(BF16)
            r.g_up[part, :] = dot(routed, r.d_up[...], 0, 0).astype(BF16)

    grads("down", 0)
    grads("down", 1)
    second(nz - 1)
    third(nz - 2, 0)
    grads("down", 2)
    grads("down", 3)
    down_out = pltpu.make_async_copy(r.g_down, r.g_down_hbm, r.own_sem.at[2])
    down_out.start()
    third(nz - 1, 0)
    for q in range(NY):
        grads("both", q)
    gate_out = pltpu.make_async_copy(r.g_gate, r.g_gate_hbm, r.own_sem.at[3])
    up_out = pltpu.make_async_copy(r.g_up, r.g_up_hbm, r.own_sem.at[4])
    gate_out.start()
    up_out.start()
    settle(r.ret.at[pl.ds(0, nz * rows - 1)], r.ret_sem)

    pieces, length = r.tg.shape[1], r.tg.shape[2]
    mid = length // 2
    returned = r.ret[...].reshape(slots, quarter)
    for i in range(pieces):
        at = slice(i * length, (i + 1) * length)
        sums = dot(r.pick[:, at], returned, 0, 0)
        r.tg[y, i] = (r.cot_q[at, :].astype(F32) + sums).astype(BF16)
        block = r.tg.at[y, i]
        remote(block, block, r.tg_sem, r.t_l.at[i], right)
        remote(block, block, r.tg_sem, r.t_r.at[i], left)

    per_sp = r.gw.shape[4]
    deep_z = r.gw.shape[3]
    many = quarter // per_sp

    def mixed(q):
        return dot(
            r.tg[q].reshape(tok, quarter),
            r.ow[pl.ds(pl.multiple_of(q * quarter, quarter), quarter), :], 1, 0,
        )

    def out_part(q):
        grad = dot(r.tg[q].reshape(tok, quarter), r.mix[...], 0, 0).astype(BF16)
        for m in range(many):
            r.gw[q, m % 2, (m // 2) % nx, m // rows] = grad[m * per_sp : (m + 1) * per_sp]
        remote(r.gw.at[q, 1 - c], r.core_in.at[q], r.core_sem, r.g1.at[q], (z, x, 1 - c, y))

    def over_x(q):
        settle(r.core_in.at[q], r.g1.at[q])
        r.x_out[q] = (r.gw[q, c].astype(F32) + r.core_in[q].astype(F32)).astype(BF16)

        def x_send(j, carry):
            to = lax.rem(x + j, nx)
            remote(r.x_out.at[q, to], r.x_in.at[q, x], r.x_sem, r.g2.at[q], (z, to, c, y))
            return carry

        lax.fori_loop(1, nx, x_send, 0)

    def over_z(q):
        if nx > 1:
            settle(r.x_in.at[q, pl.ds(0, nx - 1)], r.g2.at[q])
        total = r.x_out[q, x].astype(F32)
        for j in range(1, nx):
            total = total + r.x_in[q, lax.rem(x + j, nx)].astype(F32)
        r.last_out[pl.ds(q * deep_z, deep_z)] = total.astype(BF16)

    value = mixed(y)
    out_part(y)

    def tg_onward(i, carry):
        settle(r.tg.at[y_left, i], r.t_l.at[i])
        block = r.tg.at[y_left, i, pl.ds(0, mid)]
        remote(block, block, r.tg_sem, r.u_l.at[i], right)
        settle(r.tg.at[y_right, i], r.t_r.at[i])
        block = r.tg.at[y_right, i, pl.ds(mid, mid)]
        remote(block, block, r.tg_sem, r.u_r.at[i], left)
        return carry

    lax.fori_loop(0, pieces, tg_onward, 0)
    value = value + mixed(y_left) + mixed(y_right)
    out_part(y_left)
    out_part(y_right)
    over_x(y)

    def tg_finish(i, carry):
        settle(r.tg.at[y, i, pl.ds(0, mid)], r.u_l.at[i])
        settle(r.tg.at[y, i, pl.ds(0, mid)], r.u_r.at[i])
        return carry

    lax.fori_loop(0, pieces, tg_finish, 0)
    r.dmix[...] = (value + mixed(y_far)).astype(BF16)

    pull = jnp.zeros((256, 128), F32)
    for b in reversed(range(blocks)):
        at = slice(b * BLOCK, (b + 1) * BLOCK)
        cum = r.cum[at, :]
        end = cum[BLOCK - 1 : BLOCK, :]
        asked = (r.q[at, :].astype(F32) * 0.125 * jnp.exp(cum)).astype(BF16)
        pulled = jnp.where(same, dot(r.dmix[at, :], asked, 0, 0), 0.0)
        r.pulled[b] = pulled
        pull = pull * jnp.exp(end) + pulled
    pull = pull[0:128] + pull[128:256]
    for i in range(rows):
        r.pay[i] = pull[i * span : (i + 1) * span]

    def row_send(j, carry):
        to = lax.rem(row + j, rows)
        remote(r.pay.at[to], r.row_in.at[row], r.sent.at[0], r.p1, target(nx, z, to, y))
        return carry

    lax.fori_loop(1, rows, row_send, 0)
    out_part(y_far)
    over_x(y_left)
    over_x(y_right)
    r.row_in[row] = r.pay[row]
    inside(r, blocks)
    over_x(y_far)

    settle(r.row_in.at[pl.ds(0, rows - 1)], r.p1)
    pull = jnp.zeros((span, 128), F32)
    for j in reversed(range(rows)):
        r.row_out[j] = pull
        pull = pull * jnp.exp(kept_row(j)) + r.row_in[j]
    r.z_out[...] = pull
    r.z_in[z] = pull

    def z_send(j, carry):
        to = lax.rem(z + j, nz)
        remote(r.z_out, r.z_in.at[z], r.sent.at[1], r.p2, target(nx, to, row, y))
        return carry

    lax.fori_loop(1, nz, z_send, 0)

    for q in range(NY):
        over_z(q)

    def last_send(j, carry):
        to = lax.rem(z + j, nz)
        remote(r.last_out.at[to], r.last_in.at[z], r.sent.at[5], r.g3, (to, x, c, y))
        return carry

    lax.fori_loop(1, nz, last_send, 0)

    settle(r.z_in.at[pl.ds(0, nz - 1)], r.p2)
    pull = jnp.zeros((span, 128), F32)
    mine = jnp.zeros((span, 128), F32)
    for k in reversed(range(nz)):
        mine = jnp.where(z == k, pull, mine)
        pull = pull * jnp.exp(kept_z(k)) + r.z_in[k]
    behind = jnp.zeros((1, 128), F32)
    for j in reversed(range(rows)):
        r.row_out[j] = r.row_out[j] + mine * jnp.exp(behind)
        behind = behind + kept_row(j)

    def row_back(j, carry):
        to = lax.rem(row + j, rows)
        remote(r.row_out.at[to], r.ex.at[row], r.sent.at[2], r.p3, target(nx, z, to, y))
        return carry

    lax.fori_loop(1, rows, row_back, 0)
    r.ex[row] = r.row_out[row]

    settle(r.f_ex.at[pl.ds(0, rows - 1)], r.f3)
    settle(r.ex.at[pl.ds(0, rows - 1)], r.p3)
    across(r, blocks, rows, same)

    settle(r.last_in.at[pl.ds(0, nz - 1)], r.g3)
    total = r.last_out[z].astype(F32)
    for j in range(1, nz):
        total = total + r.last_in[lax.rem(z + j, nz)].astype(F32)
    r.gout[...] = total

    settle(r.send.at[pl.ds(0, ring * rows)], r.send_sem)
    settle(r.full.at[pl.ds(0, (1 + TRAIL) * rows - 1)], r.full_sem)
    settle(r.rows.at[pl.ds(0, 3), pl.ds(0, ring * rows)], r.ring_sem)
    settle(r.part.at[pl.ds(0, 3)], r.back_sem)
    settle(r.ret.at[pl.ds(0, nz * rows - 1)], r.home_sem)
    settle(r.tg.at[pl.ds(0, 3)], r.tg_sem)
    settle(r.pay.at[pl.ds(0, rows - 1)], r.sent.at[0])
    settle(r.z_in.at[pl.ds(0, nz - 1)], r.sent.at[1])
    settle(r.ex.at[pl.ds(0, rows - 1)], r.sent.at[2])
    settle(r.f_pay.at[pl.ds(0, rows - 1)], r.f_sent.at[0])
    settle(r.f_z_in.at[pl.ds(0, nz - 1)], r.f_sent.at[1])
    settle(r.f_ex.at[pl.ds(0, rows - 1)], r.f_sent.at[2])
    settle(r.core_in, r.core_sem)
    settle(r.last_in.at[pl.ds(0, nz - 1)], r.sent.at[5])
    if nx > 1:
        settle(r.x_in.at[:, pl.ds(0, nx - 1)], r.x_sem)
    down_out.wait()
    gate_out.wait()
    up_out.wait()


def inside(r, blocks):
    head0 = lax.broadcasted_iota(jnp.int32, (BLOCK, 128), 1) < 64
    le = triangle("le")
    ge = triangle("ge").astype(BF16)
    for b in range(blocks):
        at = slice(b * BLOCK, (b + 1) * BLOCK)
        cum = r.cum[at, :]
        middle = cum[BLOCK // 2 - 1 : BLOCK // 2, :]
        up, down = jnp.exp(cum - middle), jnp.exp(middle - cum)
        q_mid = (r.q[at, :].astype(F32) * 0.125 * up).astype(BF16)
        k_mid = (r.k[at, :].astype(F32) * down).astype(BF16)
        nothing = jnp.zeros_like(q_mid)
        dq_mid = jnp.zeros((BLOCK, 128), F32)
        dk_mid = jnp.zeros((BLOCK, 128), F32)
        for h in range(2):
            cols = slice(h * 128, (h + 1) * 128)
            mine = head0 if h == 0 else jnp.logical_not(head0)
            q_one = jnp.where(mine, q_mid, nothing)
            k_one = jnp.where(mine, k_mid, nothing)
            cot = r.dmix[at, cols]
            scores = jnp.where(le, dot(q_one, k_one, 1, 1), 0.0).astype(BF16)
            d_scores = jnp.where(le, dot(cot, r.v[at, cols], 1, 1), 0.0).astype(BF16)
            dq_mid = dq_mid + dot(d_scores, k_one, 1, 0)
            dk_mid = dk_mid + dot(d_scores, q_one, 0, 0)
            r.dv_in[at, cols] = dot(scores, cot, 0, 0)
        r.dq_in[at, :] = dq_mid * up
        r.dk_in[at, :] = dk_mid * down
        r.dl_in[at, :] = spread_sum(ge, q_mid.astype(F32) * dq_mid - k_mid.astype(F32) * dk_mid)


def across(r, blocks, rows, same):
    ge = triangle("ge").astype(BF16)
    lt = triangle("lt").astype(BF16)

    def opened(ref):
        compact = jnp.concatenate([ref[i] for i in range(rows)], axis=0)
        return jnp.where(same, jnp.concatenate([compact, compact], axis=0), 0.0)

    def end_of(b):
        return jnp.exp(r.cum[(b + 1) * BLOCK - 1 : (b + 1) * BLOCK, :])

    states = [opened(r.f_ex)]
    for b in range(blocks - 1):
        states.append(states[-1] * end_of(b) + r.added[b])
    pulls = [opened(r.ex)]
    for b in reversed(range(1, blocks)):
        pulls.insert(0, pulls[0] * end_of(b) + r.pulled[b])
    for b in range(blocks):
        at = slice(b * BLOCK, (b + 1) * BLOCK)
        cum = r.cum[at, :]
        end = cum[BLOCK - 1 : BLOCK, :]
        query = r.q[at, :].astype(F32) * 0.125
        key = r.k[at, :].astype(F32)
        asked, kept = jnp.exp(cum), jnp.exp(end - cum)
        pull = pulls[b].astype(BF16)
        far_v = dot((key * kept).astype(BF16), pull, 1, 1)
        r.dv[at, :] = (r.dv_in[at, :] + far_v).astype(BF16)
        dq_far = dot(r.dmix[at, :], states[b].astype(BF16), 1, 0) * asked
        dk_far = dot(r.v[at, :], pull, 1, 0) * kept
        r.dq[at, :] = ((r.dq_in[at, :] + dq_far) * 0.125).astype(BF16)
        r.dk[at, :] = (r.dk_in[at, :] + dk_far).astype(BF16)
        carried = jnp.sum(states[b] * pulls[b], axis=0, keepdims=True) * jnp.exp(end)
        r.dl[at, :] = (
            r.dl_in[at, :] + spread_sum(ge, query * dq_far) + spread_sum(lt, key * dk_far) + carried
        )


class Refs:
    pass


def mega(ids, weights, moe, cot, gate, up, down, out_weight, mix, query, key, value, log_decay):
    nz, nx = sizes()
    rows = 2 * nx
    half = rows // 2
    tok, width = moe.shape
    quarter = width // NY
    experts = nz * rows
    per = 2 * tok // experts
    span = 128 // rows
    deep = span + 8
    per_sp = width // experts
    units = gate.shape[1]
    sem = pltpu.SemaphoreType.DMA

    def vm(*shape, dtype=BF16):
        return pltpu.VMEM(shape, dtype)

    ins = [
        "ids",
        "weights",
        "moe_hbm",
        "cot_hbm",
        "gate_hbm",
        "up_hbm",
        "down_hbm",
        "ow_hbm",
        "mix_hbm",
        "q_hbm",
        "k_hbm",
        "v_hbm",
        "ld_hbm",
    ]
    outs = {
        "g_gate_hbm": (gate.shape, BF16),
        "g_up_hbm": (up.shape, BF16),
        "g_down_hbm": (down.shape, BF16),
        "gout": ((per_sp, 256), F32),
        "dq": ((tok, 128), BF16),
        "dk": ((tok, 128), BF16),
        "dv": ((tok, 256), BF16),
        "dl": ((tok, 128), F32),
    }
    scratch = {
        "moe_q": vm(tok, quarter),
        "cot_q": vm(tok, quarter),
        "ld": vm(tok, 128, dtype=F32),
        "k": vm(tok, 128),
        "v": vm(tok, 256),
        "q": vm(tok, 128),
        "gate": vm(*gate.shape),
        "up": vm(*up.shape),
        "down": vm(*down.shape),
        "ow": vm(*out_weight.shape),
        "mix": vm(*mix.shape),
        "pick": vm(2 * tok, tok),
        "send": vm(experts, per, 2 * quarter),
        "rows": vm(NY, experts, per, 2 * quarter),
        "hidden": vm(2 * tok, units),
        "d_gate": vm(2 * tok, units),
        "d_up": vm(2 * tok, units),
        "part": vm(NY, experts, per, quarter),
        "near_l": vm(nz, half, per, quarter),
        "near_r": vm(nz, half, per, quarter),
        "sum_l": vm(nz, half, per, quarter),
        "sum_r": vm(nz, half, per, quarter),
        "last_l": vm(nz, rows, per, quarter),
        "last_r": vm(nz, rows, per, quarter),
        "done": vm(nz, rows, per, quarter),
        "ret": vm(experts, per, quarter),
        "g_gate": vm(*gate.shape),
        "g_up": vm(*up.shape),
        "g_down": vm(*down.shape),
        "tg": vm(NY, 4, tok // 4, quarter),
        "dmix": vm(tok, 256),
        "cum": vm(tok, 128, dtype=F32),
        "added": vm(tok // BLOCK, 256, 128, dtype=F32),
        "pulled": vm(tok // BLOCK, 256, 128, dtype=F32),
        "dv_in": vm(tok, 256, dtype=F32),
        "dq_in": vm(tok, 128, dtype=F32),
        "dk_in": vm(tok, 128, dtype=F32),
        "dl_in": vm(tok, 128, dtype=F32),
        "moe": vm(tok, width),
        "cot": vm(tok, width),
        "slot_weight": vm(2 * tok, 128, dtype=F32),
        "full": vm((1 + TRAIL) * rows, NY, per, 2 * quarter),
        "gw": vm(NY, 2, nx, nz // NY, per_sp, 256),
        "f_pay": vm(rows, deep, 128, dtype=F32),
        "f_row_in": vm(rows, deep, 128, dtype=F32),
        "f_z_out": vm(deep, 128, dtype=F32),
        "f_z_in": vm(nz, deep, 128, dtype=F32),
        "f_row_out": vm(rows, span, 128, dtype=F32),
        "f_ex": vm(rows, span, 128, dtype=F32),
        "pay": vm(rows, span, 128, dtype=F32),
        "row_in": vm(rows, span, 128, dtype=F32),
        "z_out": vm(span, 128, dtype=F32),
        "z_in": vm(nz, span, 128, dtype=F32),
        "row_out": vm(rows, span, 128, dtype=F32),
        "ex": vm(rows, span, 128, dtype=F32),
        "core_in": vm(NY, nx, nz // NY, per_sp, 256),
        "x_out": vm(NY, nx, nz // NY, per_sp, 256),
        "x_in": vm(NY, nx, nz // NY, per_sp, 256),
        "last_out": vm(nz, per_sp, 256),
        "last_in": vm(nz, per_sp, 256),
        "ends": vm(rows, 128, dtype=F32),
        "load_sem": sem((13,)),
        "own_sem": sem((5,)),
        "sent": sem((6,)),
        "f_sent": sem((3,)),
    }
    for name in ("send_sem", "ring_sem", "back_sem", "home_sem", "ret_sem", "tg_sem", "p1", "p2", "p3", "g3", "full_sem", "core_sem", "x_sem", "f1", "f2", "f3"):
        scratch[name] = sem
    for name in ("come", "from_l", "from_r", "far_l", "far_r", "a_l", "a_r", "b_l", "b_r"):
        scratch[name] = sem((nz,))
    for name in ("t_l", "t_r", "u_l", "u_r", "g1", "g2"):
        scratch[name] = sem((4,))
    names = ins + list(outs) + list(scratch)

    def body(*refs):
        r = Refs()
        for name, ref in zip(names, refs):
            setattr(r, name, ref)
        mega_kernel(r, nz, nx)

    return pl.pallas_call(
        body,
        name="mega",
        out_shape=tuple(jax.ShapeDtypeStruct(*kind) for kind in outs.values()),
        in_specs=[VMEM, VMEM] + [ANY] * 11,
        out_specs=(ANY,) * 3 + (VMEM,) * 5,
        scratch_shapes=list(scratch.values()),
        compiler_params=params(1),
    )(ids, weights, moe, cot, gate, up, down, out_weight, mix, query, key, value, log_decay)


def finish_kernel(*refs):
    count = (len(refs) - 1) // 3
    sources, results, held, sem = (
        refs[:count],
        refs[count : 2 * count],
        refs[2 * count : 3 * count],
        refs[-1],
    )
    inward = [pltpu.make_async_copy(a, b, sem.at[0, i]) for i, (a, b) in enumerate(zip(sources, held))]
    outward = [pltpu.make_async_copy(a, b, sem.at[1, i]) for i, (a, b) in enumerate(zip(held, results))]
    for copy in inward:
        copy.start()
    for one, other in zip(inward, outward):
        one.wait()
        other.start()
    for copy in outward:
        copy.wait()


def finish(arrays):
    shapes = tuple(jax.ShapeDtypeStruct(a.shape, a.dtype) for a in arrays)
    return pl.pallas_call(
        finish_kernel,
        name="finish",
        out_shape=shapes,
        in_specs=[ANY] * len(arrays),
        out_specs=(ANY,) * len(arrays),
        scratch_shapes=[pltpu.VMEM(a.shape, a.dtype) for a in arrays]
        + [pltpu.SemaphoreType.DMA((2, len(arrays)))],
        compiler_params=params(),
    )(*arrays)


def shards(
    moe_input,
    cotangent,
    expert_ids,
    route_weights,
    gate_weight,
    up_weight,
    down_weight,
    out_weight,
    mixer_out,
    query_vectors,
    key_vectors,
    value_vectors,
    log_decay,
):
    results = mega(
        expert_ids.T,
        route_weights.T,
        moe_input,
        cotangent,
        gate_weight[0],
        up_weight[0],
        down_weight[0],
        out_weight,
        mixer_out,
        query_vectors,
        key_vectors,
        value_vectors,
        log_decay,
    )
    g_gate, g_up, g_down, gout, dq, dk, dv, dl = finish(results)
    return g_gate[None], g_up[None], g_down[None], gout, dq, dk, dv, dl


def solution(mesh):
    finer = Mesh(mesh.devices.reshape(8, 4, 2, mesh.shape["tp"]), ("sp_0", "sp_1", "sp_2", "tp"))
    in_specs = (
        P(SP, None),
        P(SP, None),
        P(SP, None),
        P(SP, None),
        P(SP, None, "tp"),
        P(SP, None, "tp"),
        P(SP, "tp", None),
        P(None, "tp"),
        P(SP, "tp"),
        P(SP, "tp"),
        P(SP, "tp"),
        P(SP, "tp"),
        P(SP, "tp"),
    )
    out_specs = (
        P(SP, None, "tp"),
        P(SP, None, "tp"),
        P(SP, "tp", None),
        P(SP, "tp"),
        P(SP, "tp"),
        P(SP, "tp"),
        P(SP, "tp"),
        P(SP, "tp"),
    )
    return jax.shard_map(
        shards, mesh=finer, in_specs=in_specs, out_specs=out_specs, check_vma=False
    )
```

time: 365 us -> 106 us (0.29); the launches traced: 359 us -> 106 us
  blocking collectives: 172 us -> 0 us
  Pallas kernels: 0 us -> 106 us
  other arithmetic: 56.7 us -> 0 us
  local copies, waits for them, and re-layouts: 45.6 us -> 0 us
  starting transfers between devices: 29.4 us -> 0 us
  matrix products: 27 us -> 0 us
  between operations: 14.9 us -> 0.65 us
  waiting for transfers between devices: 12.6 us -> 0 us
    all_gather x9 -> x0, blocking collectives: 131 us -> none  [the longest x6 95.8 us: entering_2(): pieces = jax.tree.map(lambda part: lax.all_gather(part, axis), total)]
    pallas_call x0 -> x2, Pallas kernels: none -> 106 us  [the longest x1 102 us: mega(): pl.pallas_call(body, name='mega', out_shape=tuple((jax.ShapeDtypeStruct(*...]
    all_to_all x1 -> x0, blocking collectives: 41.1 us -> none  [side_by_side(): lax.all_to_all(both, axis, split_axis=split_dim, concat_axis=concat_dim,...]
    all_to_all x4 -> x0, starting transfers between devices: 29.3 us -> none  [the longest x1 13.6 us: sum_at_owner(): lax.all_to_all(pieces, axis, split_axis=0, concat_axis=0, tiled=True)]
    dot_general x40 -> x0, matrix products: 27 us -> none  [the longest x12 6.27 us: block_step(): jnp.einsum('hsd,hsv->hdv', key_block * jnp.exp(final_row - cumulative), v...]
    reduce_sum x14 -> x0, other arithmetic: 20.8 us -> none  [the longest x4 16.3 us: block_step(): difference = cumulative[:, :, None, :] - cumulative[:, None, :, :]]
    while x8 -> x0, other arithmetic: 16 us -> none
    all_to_all x4 -> x0, waiting for transfers between devices: 12.6 us -> none  [the longest x1 8.25 us: sent_and_summed(): lax.all_to_all(in_blocks(shard, dim, devices), axis, 0, 0, tiled=True)]
  transfers between devices with their start and end apart: 5 -> 0, of which waited for: 2 -> 0; matrix products, arithmetic and copies ran while one was open for 27% -> 0% of each run, Pallas kernels for 0% -> 0%
where the time goes in v2:
time: 106 us
  Pallas kernels  106 us (100%)
    pallas_call x1, Pallas kernels, mega(): pl.pallas_call(body, name='mega', out_shape=tuple((jax.ShapeDtypeStruct(*...  102 us
    pallas_call x1, Pallas kernels, finish(): pl.pallas_call(finish_kernel, name='finish', out_shape=shapes, in_specs=[...  3.15 us

profile of v2, /device:TPU:1, one launch (start us, length us, event | category | flops | bytes accessed | tf_op | source)
XLA Modules:
  0.0 106.2 jit_solution(3715983942831024865)
XLA Ops:
  0.6 102.4 %mega.1 = (bf16[2048,256]{1,0:T(8,128)(2,1)}, bf16[2048,256]{1,0:T(8,128)(2,1)}, bf16[256,2048]{1,0:T(8,128)(2,1)}, f32[32,256]{1,0:T(8,128)}, bf16[256,128]{1,0...) custom-call(s32[2,256]{1,0:T(2,128)} %bitcast.11, f32[2,256]{1,0:T(2,128)} %bitcast.12, ...), custom_call_target="tpu_custom_call" | custom-call | tf_op jit(solution)/shard_map/mega/pallas_call | solution.py:860
  103.1 3.2 %finish.1 = (bf16[2048,256]{1,0:T(8,128)(2,1)}, bf16[2048,256]{1,0:T(8,128)(2,1)}, bf16[256,2048]{1,0:T(8,128)(2,1)}, f32[32,256]{1,0:T(8,128)}, bf16[256,128]{1...) custom-call(bf16[2048,256]{1,0:T(8,128)(2,1)} %get-tuple-element.24.refs_0_, ...), custom_call_target="tpu_custom_call" | custom-call | tf_op jit(solution)/shard_map/finish/pallas_call | solution.py:892

commit v3 on v2

--- a/solution.py
+++ b/solution.py
@@ -11,8 +11,8 @@
 BF16 = jnp.bfloat16
 F32 = jnp.float32
 NY = 4
-TRAIL = 2
-ORDER = {8: (0, 2, 6, 3, 5, 4, 1, 7)}
+FULL = {8: (5, 7)}
+ORDER = {8: (0, 2, 6, 3, 5, 1, 4, 7)}
 BLOCK = 64
 VMEM = pl.BlockSpec(memory_space=pltpu.VMEM)
 ANY = pl.BlockSpec(memory_space=pl.ANY)
@@ -59,29 +59,27 @@
     pltpu.make_async_copy(ref, ref, sem).wait()
 
 
-def greet_plane(barrier, nz, nx, z, row, y):
-    rows = 2 * nx
-    me = z * rows + row
-
-    def hello(i, carry):
-        far = jnp.where(i % 2 == 0, nz * rows // 2 - i // 2, nz * rows // 2 + 1 + i // 2)
-        peer = lax.rem(me + far, nz * rows)
-        pl.semaphore_signal(
-            barrier,
-            inc=1,
-            device_id=target(nx, peer // rows, lax.rem(peer, rows), y),
-            device_id_type=MESH,
-        )
+def greet_plane(barrier, nz, nx, z, x, c, y):
+    def hello(device):
+        pl.semaphore_signal(barrier, inc=1, device_id=device, device_id_type=MESH)
+
+    columns = [lax.rem(x + i, nx) for i in range(nx)]
+
+    def level(zz, own):
+        for i in reversed(range(nx)):
+            hello((zz, columns[i], 1 - c, y))
+            if i or not own:
+                hello((zz, columns[i], c, y))
+
+    def level_at(i, carry):
+        away = jnp.where(i % 2 == 0, nz // 2 - i // 2, nz // 2 + 1 + i // 2)
+        level(lax.rem(z + away, nz), False)
         return carry
 
-    lax.fori_loop(0, nz * rows - 1, hello, 0)
+    lax.fori_loop(0, nz - 1, level_at, 0)
+    level(z, True)
     for side in (1, NY - 1):
-        pl.semaphore_signal(
-            barrier,
-            inc=1,
-            device_id=target(nx, z, row, lax.rem(y + side, NY)),
-            device_id_type=MESH,
-        )
+        hello((z, x, c, lax.rem(y + side, NY)))
 
 
 def remote(src, dst, send_sem, recv_sem, device):
@@ -136,6 +134,8 @@
         pltpu.make_async_copy(src, dst, r.load_sem.at[i])
         for i, (src, dst) in enumerate(
             (
+                (r.ids_hbm, r.ids),
+                (r.weights_hbm, r.weights),
                 (r.moe_hbm.at[:, cols], r.moe_q),
                 (r.cot_hbm.at[:, cols], r.cot_q),
                 (r.ld_hbm, r.ld),
@@ -152,11 +152,15 @@
             )
         )
     ]
-    for load in loads:
+    for load in loads[:4]:
         load.start()
     barrier = pltpu.get_barrier_semaphore()
-    greet_plane(barrier, nz, nx, z, row, y)
-
+    greet_plane(barrier, nz, nx, z, x, c, y)
+
+    for load in loads[4:]:
+        load.start()
+    for load in loads[:2]:
+        load.wait()
     lanes = max(128, experts)
     which = lax.broadcasted_iota(jnp.int32, (lanes, tok), 0)
     hot = [(r.ids[j : j + 1, :] == which).astype(F32) for j in range(2)]
@@ -178,10 +182,10 @@
         chosen = picks[j].astype(F32) * r.weights[j : j + 1, :]
         slot_weight = slot_weight + jnp.sum(chosen, axis=1, keepdims=True)
     r.slot_weight[...] = jnp.broadcast_to(slot_weight, (slots, 128))
-    loads[0].wait()
+    loads[2].wait()
     sorted_rows = dot(both, r.moe_q[...], 1, 0).astype(BF16)
     r.send[:, :, 0:quarter] = sorted_rows.reshape(experts, per, quarter)
-    loads[1].wait()
+    loads[3].wait()
     sorted_cot = (dot(both, r.cot_q[...], 1, 0) * slot_weight).astype(BF16)
     r.send[:, :, quarter:] = sorted_cot.reshape(experts, per, quarter)
     pl.semaphore_wait(barrier, nz * rows + 1)
@@ -199,12 +203,13 @@
         )
         return carry
 
-    ring = nz - 1 - TRAIL
-    lax.fori_loop(rows, (ring + 1) * rows, scatter, 0)
+    own = pltpu.make_async_copy(r.send.at[me], r.rows.at[y, row], r.own_sem.at[0])
+    own.start()
+    wide = FULL.get(nz, (nz - 1,))
+    ringed = [k for k in range(nz) if k not in wide]
     lines = rows * per
-    loads[11].wait()
-    loads[12].wait()
-    for i, k in enumerate([0, *range(ring + 1, nz)]):
+
+    def fill(i, k):
         zz = lax.rem(z - offset(k, nz) + nz, nz)
         there = pl.ds(pl.multiple_of(zz * lines, lines), lines)
         pick_there = r.pick[there, :]
@@ -217,7 +222,10 @@
             value = (dot(pick_there, r.cot[:, part], 1, 0) * weight_there).astype(BF16)
             r.full[block, q, :, quarter:] = value.reshape(rows, per, quarter)
 
-        def scatter_full(j, carry, i=i, k=k, zz=zz):
+    def scatter_full(i, k):
+        zz = lax.rem(z - offset(k, nz) + nz, nz)
+
+        def one(j, carry):
             to = lax.rem(row + j, rows)
             remote(
                 r.full.at[i * rows + to],
@@ -228,15 +236,32 @@
             )
             return carry
 
-        lax.fori_loop(0 if i else 1, rows, scatter_full, 0)
-    own = pltpu.make_async_copy(r.full.at[row], r.rows.at[:, row], r.own_sem.at[0])
-    own.start()
+        lax.fori_loop(0, rows, one, 0)
+
+    begin = 1
+    for i, k in enumerate(wide):
+        lax.fori_loop(begin, k * rows, scatter, 0)
+        if i == 0:
+            loads[13].wait()
+            loads[14].wait()
+            for ii, kk in enumerate(wide):
+                fill(ii, kk)
+        scatter_full(i, k)
+        begin = (k + 1) * rows
+    if begin < nz * rows:
+        lax.fori_loop(begin, nz * rows, scatter, 0)
     own.wait()
+
+    def is_ring(k):
+        answer = k >= 0
+        for w in wide:
+            answer = answer & (k != w)
+        return answer
 
     blocks = tok // BLOCK
     same = diagonal((256, 128))
     tri = triangle("le").astype(BF16)
-    for load in loads[2:5]:
+    for load in loads[4:7]:
         load.wait()
     state = jnp.zeros((256, 128), F32)
     for b in range(blocks):
@@ -307,7 +332,7 @@
         lax.fori_loop(1, rows, send, 0)
         r.f_ex[row] = r.f_row_out[row]
 
-    for load in loads[5:11]:
+    for load in loads[7:13]:
         load.wait()
 
     def chunk(k):
@@ -409,26 +434,25 @@
         settle(r.rows.at[y, pl.ds(0, rows)], r.come.at[k])
         spread(k)
 
+    settle(r.rows.at[y, pl.ds(0, rows - 1)], r.come.at[0])
+    spread(0)
     arrive(1)
+    onward(0)
 
     def step(t, carry):
-        @pl.when(t + 1 <= ring)
+        @pl.when(is_ring(t + 1) & (t + 1 < nz))
         def _():
             arrive(t + 1)
 
-        @pl.when(t <= ring)
+        @pl.when(is_ring(t) & (t < nz))
         def _():
             onward(t)
 
-        @pl.when(t == 1)
-        def _():
-            settle(r.rows.at[0, pl.ds(0, NY * (rows - 1))], r.come.at[0])
-
-        @pl.when((t > 1) & (t <= ring + 1))
+        @pl.when(is_ring(t - 1))
         def _():
             gathered(t - 1)
 
-        @pl.when(t > ring + 1)
+        @pl.when(jnp.logical_not(is_ring(t - 1)))
         def _():
             settle(r.rows.at[0, pl.ds(0, NY * rows)], r.come.at[t - 1])
 
@@ -479,15 +503,9 @@
     third(nz - 2, 0)
     grads("down", 2)
     grads("down", 3)
-    down_out = pltpu.make_async_copy(r.g_down, r.g_down_hbm, r.own_sem.at[2])
-    down_out.start()
     third(nz - 1, 0)
     for q in range(NY):
         grads("both", q)
-    gate_out = pltpu.make_async_copy(r.g_gate, r.g_gate_hbm, r.own_sem.at[3])
-    up_out = pltpu.make_async_copy(r.g_up, r.g_up_hbm, r.own_sem.at[4])
-    gate_out.start()
-    up_out.start()
     settle(r.ret.at[pl.ds(0, nz * rows - 1)], r.ret_sem)
 
     pieces, length = r.tg.shape[1], r.tg.shape[2]
@@ -585,8 +603,6 @@
     over_x(y_left)
     over_x(y_right)
     r.row_in[row] = r.pay[row]
-    inside(r, blocks)
-    over_x(y_far)
 
     settle(r.row_in.at[pl.ds(0, rows - 1)], r.p1)
     pull = jnp.zeros((span, 128), F32)
@@ -602,6 +618,8 @@
         return carry
 
     lax.fori_loop(1, nz, z_send, 0)
+    over_x(y_far)
+    inside(r, blocks)
 
     for q in range(NY):
         over_z(q)
@@ -642,9 +660,9 @@
         total = total + r.last_in[lax.rem(z + j, nz)].astype(F32)
     r.gout[...] = total
 
-    settle(r.send.at[pl.ds(0, ring * rows)], r.send_sem)
-    settle(r.full.at[pl.ds(0, (1 + TRAIL) * rows - 1)], r.full_sem)
-    settle(r.rows.at[pl.ds(0, 3), pl.ds(0, ring * rows)], r.ring_sem)
+    settle(r.send.at[pl.ds(0, len(ringed) * rows - 1)], r.send_sem)
+    settle(r.full, r.full_sem)
+    settle(r.rows.at[pl.ds(0, 3), pl.ds(0, len(ringed) * rows)], r.ring_sem)
     settle(r.part.at[pl.ds(0, 3)], r.back_sem)
     settle(r.ret.at[pl.ds(0, nz * rows - 1)], r.home_sem)
     settle(r.tg.at[pl.ds(0, 3)], r.tg_sem)
@@ -658,9 +676,6 @@
     settle(r.last_in.at[pl.ds(0, nz - 1)], r.sent.at[5])
     if nx > 1:
         settle(r.x_in.at[:, pl.ds(0, nx - 1)], r.x_sem)
-    down_out.wait()
-    gate_out.wait()
-    up_out.wait()
 
 
 def inside(r, blocks):
@@ -752,8 +767,8 @@
         return pltpu.VMEM(shape, dtype)
 
     ins = [
-        "ids",
-        "weights",
+        "ids_hbm",
+        "weights_hbm",
         "moe_hbm",
         "cot_hbm",
         "gate_hbm",
@@ -767,9 +782,9 @@
         "ld_hbm",
     ]
     outs = {
-        "g_gate_hbm": (gate.shape, BF16),
-        "g_up_hbm": (up.shape, BF16),
-        "g_down_hbm": (down.shape, BF16),
+        "g_gate": (gate.shape, BF16),
+        "g_up": (up.shape, BF16),
+        "g_down": (down.shape, BF16),
         "gout": ((per_sp, 256), F32),
         "dq": ((tok, 128), BF16),
         "dk": ((tok, 128), BF16),
@@ -777,6 +792,8 @@
         "dl": ((tok, 128), F32),
     }
     scratch = {
+        "ids": vm(2, tok, dtype=jnp.int32),
+        "weights": vm(2, tok, dtype=F32),
         "moe_q": vm(tok, quarter),
         "cot_q": vm(tok, quarter),
         "ld": vm(tok, 128, dtype=F32),
@@ -803,9 +820,6 @@
         "last_r": vm(nz, rows, per, quarter),
         "done": vm(nz, rows, per, quarter),
         "ret": vm(experts, per, quarter),
-        "g_gate": vm(*gate.shape),
-        "g_up": vm(*up.shape),
-        "g_down": vm(*down.shape),
         "tg": vm(NY, 4, tok // 4, quarter),
         "dmix": vm(tok, 256),
         "cum": vm(tok, 128, dtype=F32),
@@ -818,7 +832,7 @@
         "moe": vm(tok, width),
         "cot": vm(tok, width),
         "slot_weight": vm(2 * tok, 128, dtype=F32),
-        "full": vm((1 + TRAIL) * rows, NY, per, 2 * quarter),
+        "full": vm(len(FULL.get(nz, (1,))) * rows, NY, per, 2 * quarter),
         "gw": vm(NY, 2, nx, nz // NY, per_sp, 256),
         "f_pay": vm(rows, deep, 128, dtype=F32),
         "f_row_in": vm(rows, deep, 128, dtype=F32),
@@ -838,8 +852,8 @@
         "last_out": vm(nz, per_sp, 256),
         "last_in": vm(nz, per_sp, 256),
         "ends": vm(rows, 128, dtype=F32),
-        "load_sem": sem((13,)),
-        "own_sem": sem((5,)),
+        "load_sem": sem((15,)),
+        "own_sem": sem((2,)),
         "sent": sem((6,)),
         "f_sent": sem((3,)),
     }
@@ -860,30 +874,23 @@
     return pl.pallas_call(
         body,
         name="mega",
-        out_shape=tuple(jax.ShapeDtypeStruct(*kind) for kind in outs.values()),
-        in_specs=[VMEM, VMEM] + [ANY] * 11,
-        out_specs=(ANY,) * 3 + (VMEM,) * 5,
+        out_shape=tuple(pltpu.VMEM(*kind) for kind in outs.values()),
+        in_specs=[pl.BlockSpec(memory_space=pltpu.HBM)] * 13,
+        out_specs=(VMEM,) * 8,
         scratch_shapes=list(scratch.values()),
         compiler_params=params(1),
     )(ids, weights, moe, cot, gate, up, down, out_weight, mix, query, key, value, log_decay)
 
 
 def finish_kernel(*refs):
-    count = (len(refs) - 1) // 3
-    sources, results, held, sem = (
-        refs[:count],
-        refs[count : 2 * count],
-        refs[2 * count : 3 * count],
-        refs[-1],
-    )
-    inward = [pltpu.make_async_copy(a, b, sem.at[0, i]) for i, (a, b) in enumerate(zip(sources, held))]
-    outward = [pltpu.make_async_copy(a, b, sem.at[1, i]) for i, (a, b) in enumerate(zip(held, results))]
-    for copy in inward:
+    count = (len(refs) - 1) // 2
+    sem = refs[-1]
+    copies = [
+        pltpu.make_async_copy(refs[i], refs[count + i], sem.at[i]) for i in range(count)
+    ]
+    for copy in copies:
         copy.start()
-    for one, other in zip(inward, outward):
-        one.wait()
-        other.start()
-    for copy in outward:
+    for copy in copies:
         copy.wait()
 
 
@@ -893,12 +900,11 @@
         finish_kernel,
         name="finish",
         out_shape=shapes,
-        in_specs=[ANY] * len(arrays),
+        in_specs=[VMEM] * len(arrays),
         out_specs=(ANY,) * len(arrays),
-        scratch_shapes=[pltpu.VMEM(a.shape, a.dtype) for a in arrays]
-        + [pltpu.SemaphoreType.DMA((2, len(arrays)))],
-        compiler_params=params(),
-    )(*arrays)
+        scratch_shapes=[pltpu.SemaphoreType.DMA((len(arrays),))],
+        compiler_params=pltpu.CompilerParams(vmem_limit_bytes=1024 * 1024),
+    )(*[pltpu.with_memory_space_constraint(a, pltpu.VMEM) for a in arrays])
 
 
 def shards(

time: 106 us -> 104 us (0.981)
  Pallas kernels: 106 us -> 103 us
    pallas_call x1, Pallas kernels: 102 us -> 101 us  [mega(): pl.pallas_call(body, name='mega', out_shape=tuple((pltpu.VMEM(*kind) for...]
    pallas_call x1, Pallas kernels: 3.15 us -> 1.86 us  [finish(): pl.pallas_call(finish_kernel, name='finish', out_shape=shapes, in_specs=[...]
where the time goes in v3:
time: 104 us
  Pallas kernels  103 us (99%)
    pallas_call x1, Pallas kernels, mega(): pl.pallas_call(body, name='mega', out_shape=tuple((pltpu.VMEM(*kind) for...  101 us

profile of v3, /device:TPU:1, one launch (start us, length us, event | category | flops | bytes accessed | tf_op | source)
XLA Modules:
  0.0 103.5 jit_solution(4686199820697903575)
XLA Ops:
  0.6 101.0 %mega.1 = (bf16[2048,256]{1,0:T(8,128)(2,1)S(1)}, bf16[2048,256]{1,0:T(8,128)(2,1)S(1)}, bf16[256,2048]{1,0:T(8,128)(2,1)S(1)}, f32[32,256]{1,0:T(8,128)S(1)}, b...) custom-call(s32[2,256]{1,0:T(2,128)} %bitcast.11, ...), custom_call_target="tpu_custom_call" | custom-call | tf_op jit(solution)/shard_map/mega/pallas_call | solution.py:874
  101.7 1.9 %finish.1 = (bf16[2048,256]{1,0:T(8,128)(2,1)}, bf16[2048,256]{1,0:T(8,128)(2,1)}, bf16[256,2048]{1,0:T(8,128)(2,1)}, f32[32,256]{1,0:T(8,128)}, bf16[256,128]{1...) custom-call(bf16[2048,256]{1,0:T(8,128)(2,1)S(1)} %get-tuple-element.24.refs_0_, ...), custom_call_target="tpu_custom_call" | custom-call | tf_op jit(solution)/shard_map/finish/pallas_call | solution.py:899

commit v4 on v3

--- a/solution.py
+++ b/solution.py
@@ -621,16 +621,6 @@
     over_x(y_far)
     inside(r, blocks)
 
-    for q in range(NY):
-        over_z(q)
-
-    def last_send(j, carry):
-        to = lax.rem(z + j, nz)
-        remote(r.last_out.at[to], r.last_in.at[z], r.sent.at[5], r.g3, (to, x, c, y))
-        return carry
-
-    lax.fori_loop(1, nz, last_send, 0)
-
     settle(r.z_in.at[pl.ds(0, nz - 1)], r.p2)
     pull = jnp.zeros((span, 128), F32)
     mine = jnp.zeros((span, 128), F32)
@@ -649,6 +639,16 @@
 
     lax.fori_loop(1, rows, row_back, 0)
     r.ex[row] = r.row_out[row]
+
+    for q in range(NY):
+        over_z(q)
+
+    def last_send(j, carry):
+        to = lax.rem(z + j, nz)
+        remote(r.last_out.at[to], r.last_in.at[z], r.sent.at[5], r.g3, (to, x, c, y))
+        return carry
+
+    lax.fori_loop(1, nz, last_send, 0)
 
     settle(r.f_ex.at[pl.ds(0, rows - 1)], r.f3)
     settle(r.ex.at[pl.ds(0, rows - 1)], r.p3)
@@ -820,7 +820,7 @@
         "last_r": vm(nz, rows, per, quarter),
         "done": vm(nz, rows, per, quarter),
         "ret": vm(experts, per, quarter),
-        "tg": vm(NY, 4, tok // 4, quarter),
+        "tg": vm(NY, 8, tok // 8, quarter),
         "dmix": vm(tok, 256),
         "cum": vm(tok, 128, dtype=F32),
         "added": vm(tok // BLOCK, 256, 128, dtype=F32),
@@ -862,7 +862,7 @@
     for name in ("come", "from_l", "from_r", "far_l", "far_r", "a_l", "a_r", "b_l", "b_r"):
         scratch[name] = sem((nz,))
     for name in ("t_l", "t_r", "u_l", "u_r", "g1", "g2"):
-        scratch[name] = sem((4,))
+        scratch[name] = sem((8,))
     names = ins + list(outs) + list(scratch)
 
     def body(*refs):

time: 104 us -> 104 us (level)
  no operation moved by 1% of the time
where the time goes in v4:
time: 104 us
  Pallas kernels  103 us (99%)
    pallas_call x1, Pallas kernels, mega(): pl.pallas_call(body, name='mega', out_shape=tuple((pltpu.VMEM(*kind) for...  101 us

profile of v4, /device:TPU:1, one launch (start us, length us, event | category | flops | bytes accessed | tf_op | source)
XLA Modules:
  0.0 103.7 jit_solution(579229522634611668)
XLA Ops:
  0.6 101.2 %mega.1 = (bf16[2048,256]{1,0:T(8,128)(2,1)S(1)}, bf16[2048,256]{1,0:T(8,128)(2,1)S(1)}, bf16[256,2048]{1,0:T(8,128)(2,1)S(1)}, f32[32,256]{1,0:T(8,128)S(1)}, b...) custom-call(s32[2,256]{1,0:T(2,128)} %bitcast.11, ...), custom_call_target="tpu_custom_call" | custom-call | tf_op jit(solution)/shard_map/mega/pallas_call | solution.py:874
  101.8 1.9 %finish.1 = (bf16[2048,256]{1,0:T(8,128)(2,1)}, bf16[2048,256]{1,0:T(8,128)(2,1)}, bf16[256,2048]{1,0:T(8,128)(2,1)}, f32[32,256]{1,0:T(8,128)}, bf16[256,128]{1...) custom-call(bf16[2048,256]{1,0:T(8,128)(2,1)S(1)} %get-tuple-element.24.refs_0_, ...), custom_call_target="tpu_custom_call" | custom-call | tf_op jit(solution)/shard_map/finish/pallas_call | solution.py:899
